TPU v7x, 32 devices: a whole 2x2x4 slice. The times are simulated.
32 devices in a mesh: sp: 8 (over z, y), tp: 4 (over x, core).
Axes of the slice: x: 2, y: 2, z: 4, core: 2. Of those that a mesh axis runs over, the one named last changes fastest.
Arguments:
- tokens: bfloat16 [4096, 2048], P(('sp', 'tp')), may hold values from -6 to 6
- pooling_input_weight: bfloat16 [2048, 1024], P('sp', 'tp'), may hold values from -0.125 to 0.125
- query_matrix: bfloat16 [2048, 512], P('sp', 'tp'), may hold values from -0.125 to 0.125
- key_matrix: bfloat16 [2048, 512], P('sp', 'tp'), may hold values from -0.125 to 0.125
- value_matrix: bfloat16 [2048, 1024], P('sp', 'tp'), may hold values from -0.125 to 0.125
- decay_inner_weight: bfloat16 [2048, 64], replicated, may hold values from -0.125 to 0.125
- decay_outer_weight: bfloat16 [2, 32, 512], replicated, may hold values from -1 to 1
- channel_decay_bias: float32 [2, 512], replicated, may hold values from -0.3 to 12
- spike_log_decay: float32 [8, 4096], P('tp', 'sp'), may hold values from -0.72 to 0
- starting_state: float32 [2, 8, 64, 128], P(None, 'tp'), may hold values from -96 to 96
- pooling_group_map: bfloat16 [4, 256, 256], replicated, may hold values from -0.375 to 0.375
- pooling_output_weight: bfloat16 [1024, 2048], P('tp', 'sp'), may hold values from -0.125 to 0.125
- attention_output_weight: bfloat16 [1024, 2048], P('tp', 'sp'), may hold values from -0.125 to 0.125
Outputs:
- mixed: bfloat16 [4096, 2048], P(('sp', 'tp'))
All inputs are finite; a program needn't handle non-finite values.
Results may differ from a plain program's by a relative error of at most 0.015.
Values may be sent and summed in bfloat16 or wider, within the bound.
A program may use at most 64 MiB of HBM per device.

v0:
```python
import functools

import jax
import jax.numpy as jnp
from jax import lax
from jax.experimental import pallas as pl
from jax.experimental.pallas import tpu as pltpu
from jax.sharding import PartitionSpec as P

KEY_CHANNELS = 64
DV = 128
RANK = 32
BLOCK = 64


eps_value = 1e-06
gate_norm_factor = 16.0
highest = lax.Precision.HIGHEST
rim_width = 8


def extended(value, sides, width):
    for axis, dim in sides:
        devices, length = (lax.axis_size(axis), value.shape[dim])
        up = [(i, (i + 1) % devices) for i in range(devices - 1)]
        down = [(j, i) for i, j in up]
        last = lax.slice_in_dim(value, length - width, length, axis=dim)
        leading = lax.slice_in_dim(value, 0, width, axis=dim)
        before = lax.ppermute(last, axis, up)
        after = lax.ppermute(leading, axis, down)
        value = jnp.concatenate([before, value, after], axis=dim)
    return value


def entering_2(value, axis, join, neutral, backward):
    count = lax.axis_size(axis)
    place = lax.axis_index(axis)
    ahead = count - 1 - place if backward else place
    gathered = jax.tree.map(
        lambda a, kind: lax.all_gather(a.astype(kind), axis),
        value,
        jax.tree.map(lambda a: jnp.bfloat16 if a.dtype == jnp.float32 else a.dtype, value),
    )
    state = jax.tree.map(lambda a, e: jnp.zeros_like(a) + jnp.asarray(e, a.dtype), value, neutral)

    def one(lap, state):
        source = count - 1 - lap if backward else lap
        return join(
            state,
            jax.tree.map(
                lambda a, own: lax.dynamic_index_in_dim(a, source, 0, False).astype(own.dtype),
                gathered,
                value,
            ),
        )

    return lax.fori_loop(0, ahead, one, state)


def normalize(token_rows):
    floats = token_rows.astype(jnp.float32)
    scaled = floats * lax.rsqrt(jnp.mean(floats * floats, axis=-1, keepdims=True) + eps_value)
    return scaled.astype(jnp.bfloat16)


def chain_combine(earlier, later):
    return (earlier[0] + later[0], jnp.exp(later[0])[..., None] * earlier[1] + later[1])


def local_chain(decays, updates, backward):

    def advance(carried, element):
        log_total, memory = carried
        decay_now, update_now = element
        return (
            (log_total + decay_now, jnp.exp(decay_now)[..., None] * memory + update_now),
            (log_total, memory),
        )

    begin = (jnp.zeros_like(decays[0]), jnp.zeros_like(updates[0]))
    return lax.scan(advance, begin, (decays, updates), reverse=backward)


def within_blocks(queries, cumulative, key_rows, value_rows, lower):
    row_ids = lax.broadcasted_iota(jnp.int32, (BLOCK, BLOCK), 0)
    col_ids = lax.broadcasted_iota(jnp.int32, (BLOCK, BLOCK), 1)
    allowed = col_ids <= row_ids if lower else col_ids > row_ids
    scaled_q = queries * jnp.exp(cumulative)
    scaled_k = key_rows * jnp.exp(-cumulative)
    scores = jnp.einsum("hnid,hnjd->hnij", scaled_q, scaled_k, precision=highest)
    scores = jnp.where(allowed, scores, 0.0)
    return (scaled_q, jnp.einsum("hnij,hnjv->hniv", scores, value_rows, precision=highest))


def block_updates(key_rows, value_rows, cumulative, edge):
    weighted = key_rows * jnp.exp(edge[:, :, None, :] - cumulative)
    return jnp.einsum("hncd,hncv->hndv", weighted, value_rows, precision=highest)


def carried_term(scaled_q, before, entering):
    log_before, memory_before = before
    block_memory = jnp.exp(log_before)[..., None] * entering[None] + memory_before
    return jnp.einsum("hnid,nhdv->hniv", scaled_q, block_memory, precision=highest)


def shards(
    tokens,
    pooling_input_weight,
    query_matrix,
    key_matrix,
    value_matrix,
    decay_inner_weight,
    decay_outer_weight,
    channel_decay_bias,
    spike_log_decay,
    starting_state,
    pooling_group_map,
    pooling_output_weight,
    attention_output_weight,
):
    sp_index = lax.axis_index("sp")
    tp_index = lax.axis_index("tp")
    normed = normalize(tokens)
    pool_cols = pooling_input_weight.shape[1]
    qk_cols = query_matrix.shape[1]
    value_cols = value_matrix.shape[1]
    local_weight = jnp.concatenate(
        [pooling_input_weight, query_matrix, key_matrix, value_matrix], axis=1
    )
    whole_weight = lax.all_gather(local_weight, "sp", axis=0, tiled=True)
    row_piece = lax.all_gather(normed, "tp", axis=0, tiled=True)
    main_part = jnp.dot(row_piece, whole_weight, preferred_element_type=jnp.float32).astype(
        jnp.bfloat16
    )
    rank_part = jnp.dot(row_piece, decay_inner_weight, preferred_element_type=jnp.float32).astype(
        jnp.bfloat16
    )
    projected = jnp.concatenate([main_part, rank_part], axis=1)
    sequence_length = projected.shape[0]
    blocks = sequence_length // BLOCK
    heads_here = qk_cols // KEY_CHANNELS
    pool_input = projected[:, :pool_cols]
    query_part = projected[:, pool_cols : pool_cols + qk_cols]
    key_part = projected[:, pool_cols + qk_cols : pool_cols + 2 * qk_cols]
    value_part = projected[:, pool_cols + 2 * qk_cols : pool_cols + 2 * qk_cols + value_cols]
    low_rank = projected[:, pool_cols + 2 * qk_cols + value_cols :]
    window = jnp.left_shift(jnp.int32(2), tp_index)
    half_width = window // 2
    padded = extended(pool_input, (("sp", 0),), rim_width)
    floats = padded.astype(jnp.float32)
    window_sum = jnp.zeros((sequence_length, pool_cols), jnp.float32)
    for offset in range(-rim_width, rim_width):
        inside = ((offset >= -half_width) & (offset < window - half_width)).astype(jnp.float32)
        window_sum = (
            window_sum + inside * floats[rim_width + offset : rim_width + offset + sequence_length]
        )
    seq_length = sequence_length * lax.axis_size("sp")
    position = sp_index * sequence_length + jnp.arange(sequence_length, dtype=jnp.int32)
    low_end = jnp.clip(position - half_width, 0, seq_length - 1)
    high_end = jnp.clip(position - half_width + window - 1, 0, seq_length - 1)
    counted = (high_end - low_end + 1).astype(jnp.float32)[:, None]
    pooled = (window_sum / counted - floats[rim_width : rim_width + sequence_length]).astype(
        jnp.bfloat16
    )
    mix_here = lax.dynamic_index_in_dim(pooling_group_map, tp_index, 0, keepdims=False)
    pool_output = jnp.dot(pooled, mix_here, preferred_element_type=jnp.float32).astype(jnp.bfloat16)

    def split_heads(token_level, width):
        return (
            token_level.astype(jnp.float32)
            .reshape(blocks, BLOCK, heads_here, width)
            .transpose(2, 0, 1, 3)
        )

    queries = split_heads(query_part, KEY_CHANNELS) * KEY_CHANNELS ** (-0.5)
    key_rows = split_heads(key_part, KEY_CHANNELS)
    value_rows = split_heads(value_part, DV)
    up_here = lax.dynamic_slice_in_dim(decay_outer_weight, tp_index * qk_cols, qk_cols, 2)
    bias_here = lax.dynamic_slice_in_dim(channel_decay_bias, tp_index * qk_cols, qk_cols, 1)
    spike_amounts = spike_log_decay.T[:, :, None]

    def log_decay(direction):
        preactivation = (
            jnp.dot(
                low_rank[:, direction * RANK : (direction + 1) * RANK],
                up_here[direction],
                preferred_element_type=jnp.float32,
            )
            + bias_here[direction]
        )
        token_level = (jax.nn.log_sigmoid(preactivation) / gate_norm_factor).reshape(
            sequence_length, heads_here, KEY_CHANNELS
        ) + spike_amounts
        return token_level.reshape(blocks, BLOCK, heads_here, KEY_CHANNELS).transpose(2, 0, 1, 3)

    cum_fwd = jnp.cumsum(log_decay(0), axis=2)
    cum_bwd = jnp.flip(jnp.cumsum(jnp.flip(log_decay(1), 2), axis=2), 2)
    scaled_fwd, inner_fwd = within_blocks(queries, cum_fwd, key_rows, value_rows, True)
    scaled_bwd, inner_bwd = within_blocks(queries, cum_bwd, key_rows, value_rows, False)
    edge_fwd = cum_fwd[:, :, -1, :]
    edge_bwd = cum_bwd[:, :, 0, :]
    updates_fwd = block_updates(key_rows, value_rows, cum_fwd, edge_fwd)
    updates_bwd = block_updates(key_rows, value_rows, cum_bwd, edge_bwd)
    total_fwd, before_fwd = local_chain(
        jnp.moveaxis(edge_fwd, 1, 0), jnp.moveaxis(updates_fwd, 1, 0), False
    )
    total_bwd, before_bwd = local_chain(
        jnp.moveaxis(edge_bwd, 1, 0), jnp.moveaxis(updates_bwd, 1, 0), True
    )
    neutral = (jnp.zeros_like(total_fwd[0]), jnp.zeros_like(total_fwd[1]))
    prefix_fwd = entering_2(total_fwd, "sp", chain_combine, neutral, False)
    prefix_bwd = entering_2(total_bwd, "sp", chain_combine, neutral, True)
    entering_fwd = jnp.exp(prefix_fwd[0])[..., None] * starting_state[0] + prefix_fwd[1]
    entering_bwd = jnp.exp(prefix_bwd[0])[..., None] * starting_state[1] + prefix_bwd[1]
    out_fwd = inner_fwd + carried_term(scaled_fwd, before_fwd, entering_fwd)
    out_bwd = inner_bwd + carried_term(scaled_bwd, before_bwd, entering_bwd)
    joined = out_fwd + out_bwd
    normal_scale = lax.rsqrt(jnp.mean(joined * joined, axis=-1, keepdims=True) + eps_value)
    attention_output = (
        (joined * normal_scale)
        .astype(jnp.bfloat16)
        .transpose(1, 2, 0, 3)
        .reshape(sequence_length, heads_here * DV)
    )
    whole_pool, whole_attention = (
        lax.all_gather(pooling_output_weight, "sp", axis=1, tiled=True),
        lax.all_gather(attention_output_weight, "sp", axis=1, tiled=True),
    )
    part_one = jnp.dot(pool_output, whole_pool, preferred_element_type=jnp.float32)
    part_two = jnp.dot(attention_output, whole_attention, preferred_element_type=jnp.float32)
    return lax.psum_scatter(
        (part_one + part_two).astype(jnp.bfloat16), "tp", scatter_dimension=0, tiled=True
    )


MESH = pl.DeviceIdType.MESH
IN_CHUNKS = 3
OUT_CHUNKS = 4
RIM = 16
X_CHUNKS = 4
EARLY = (0, 0, 1, 1, 1, 1, 1)


def nt(a, b):
    return lax.dot_general(a, b, (((1,), (1,)), ((), ())), preferred_element_type=jnp.float32)


def tn(a, b):
    return lax.dot_general(a, b, (((0,), (0,)), ((), ())), preferred_element_type=jnp.float32)


def nn(a, b):
    return jnp.dot(a, b, preferred_element_type=jnp.float32)


def fused(
    n,
    tokens,
    w_pool,
    w_query,
    w_key,
    w_value,
    inner,
    outer,
    bias,
    spikes,
    start,
    group_map,
    w_pool_out,
    w_att_out,
    result,
    xraw,
    normed,
    wbuf,
    obuf,
    pbuf,
    qkv,
    ld,
    qbuf,
    upd,
    edges,
    before_b,
    acc,
    act,
    msg,
    inbox,
    gmap,
    sib_out,
    sib_in,
    x_out,
    x_in,
    own,
    local_sem,
    tok_send,
    tok_recv,
    in_send,
    in_recv,
    out_send,
    out_recv,
    halo_send,
    halo_recv,
    st_send,
    st_recv,
    sib_send,
    sib_recv,
    x_send,
    x_recv,
):
    me = lax.axis_index("sp")
    tp = lax.axis_index("tp")
    m = tokens.shape[0]
    tps = normed.shape[0] // m
    seq = normed.shape[0]
    rows = w_pool.shape[0]
    pc, qc, vc = w_pool.shape[1], w_query.shape[1], w_value.shape[1]
    width = pc + 2 * qc + vc
    blocks = seq // BLOCK
    half = n // 2
    f32, bf16 = jnp.float32, jnp.bfloat16

    odd = lax.rem(me, 2)
    pos = jnp.where(odd == 0, me // 2, n - 1 - me // 2)

    def at_pos(p):
        p = lax.rem(p + 2 * n, n)
        return jnp.where(p < half, 2 * p, 2 * (n - 1 - p) + 1)

    nexts = (at_pos(pos + 1), at_pos(pos - 1))

    locals_ = []

    def local(src, dst):
        copy = pltpu.make_async_copy(src, dst, local_sem.at[len(locals_)])
        copy.start()
        locals_.append(copy)
        return copy

    my_rows = pl.ds(pl.multiple_of(me * rows, rows), rows)
    w_copies = [
        local(w_pool, wbuf.at[my_rows, pl.ds(0, pc)]),
        local(w_query, wbuf.at[my_rows, pl.ds(pc, qc)]),
        local(w_key, wbuf.at[my_rows, pl.ds(pc + qc, qc)]),
        local(w_value, wbuf.at[my_rows, pl.ds(pc + 2 * qc, vc)]),
    ]
    o_copies = [
        local(w_pool_out, obuf.at[me, pl.ds(0, pc)]),
        local(w_att_out, obuf.at[me, pl.ds(pc, vc)]),
    ]
    my_tok = pl.ds(pl.multiple_of(tp * m, m), m)
    t_copy = local(tokens, xraw.at[my_tok])
    g_copy = local(group_map.at[tp], gmap)

    barrier = pltpu.get_barrier_semaphore()
    for d in range(1, n):
        pl.semaphore_signal(
            barrier, inc=1, device_id={"sp": lax.rem(me + d, n)}, device_id_type=MESH
        )
    for d in range(1, tps):
        pl.semaphore_signal(
            barrier, inc=1, device_id={"tp": lax.rem(tp + d, tps)}, device_id_type=MESH
        )
    pl.semaphore_wait(barrier, n - 1 + tps - 1)

    def token_copy(d):
        return pltpu.make_async_remote_copy(
            src_ref=tokens,
            dst_ref=xraw.at[my_tok],
            send_sem=tok_send.at[d - 1],
            recv_sem=tok_recv.at[d - 1],
            device_id={"tp": lax.rem(tp + d, tps)},
            device_id_type=MESH,
        )

    def in_copy(d, c, s):
        origin = at_pos(pos - s if d == 0 else pos + s)
        step = width // (2 * IN_CHUNKS)
        part = wbuf.at[
            pl.ds(pl.multiple_of(origin * rows, rows), rows),
            pl.ds((d * IN_CHUNKS + c) * step, step),
        ]
        return pltpu.make_async_remote_copy(
            src_ref=part,
            dst_ref=part,
            send_sem=in_send.at[d, c, s],
            recv_sem=in_recv.at[d, c, s],
            device_id={"sp": nexts[d]},
            device_id_type=MESH,
        )

    def in_landed(d, c, s):
        origin = at_pos(pos - s - 1 if d == 0 else pos + s + 1)
        step = width // (2 * IN_CHUNKS)
        part = wbuf.at[
            pl.ds(pl.multiple_of(origin * rows, rows), rows),
            pl.ds((d * IN_CHUNKS + c) * step, step),
        ]
        return pltpu.make_async_remote_copy(
            src_ref=part,
            dst_ref=part,
            send_sem=in_send.at[d, c, s],
            recv_sem=in_recv.at[d, c, s],
            device_id={"sp": nexts[d]},
            device_id_type=MESH,
        )

    def out_pair(d, c, s, landed):
        shift = s + 1 if landed else s
        origin = at_pos(pos - shift if d == 0 else pos + shift)
        step = (pc + vc) // (2 * OUT_CHUNKS)
        part = obuf.at[origin, pl.ds((d * OUT_CHUNKS + c) * step, step)]
        return pltpu.make_async_remote_copy(
            src_ref=part,
            dst_ref=part,
            send_sem=out_send.at[d, c, s],
            recv_sem=out_recv.at[d, c, s],
            device_id={"sp": nexts[d]},
            device_id_type=MESH,
        )

    def in_step(s):
        for c in range(IN_CHUNKS):
            for d in range(2):
                if s > 0:
                    in_landed(d, c, s - 1).wait_recv()
                if s < n - 1:
                    in_copy(d, c, s).start()

    def out_step(s):
        for c in range(OUT_CHUNKS):
            for d in range(2):
                if s > 0:
                    out_pair(d, c, s - 1, True).wait_recv()
                if s < n - 1:
                    out_pair(d, c, s, False).start()

    def normalize_piece(source):
        piece = pl.ds(pl.multiple_of(source * m, m), m)
        floats = xraw[piece, :].astype(f32)
        scale = lax.rsqrt(jnp.mean(floats * floats, axis=-1, keepdims=True) + eps_value)
        normed[piece, :] = (floats * scale).astype(bf16)

    pumped = 0

    def pump(count):
        nonlocal pumped
        for s in range(pumped, min(pumped + count, n - 1)):
            out_step(s)
            pumped = s + 1

    for copy in w_copies:
        copy.wait()
    in_step(0)
    for d in (2, 1, 3):
        token_copy(d).start()
    for copy in o_copies:
        copy.wait()
    t_copy.wait()
    g_copy.wait()
    in_step(1)
    normalize_piece(tp)
    for s in range(2, n - 1):
        in_step(s)
        pump(EARLY[s] if s < len(EARLY) else 0)
        if s in (3, 4, 5):
            d = {3: 1, 4: 3, 5: 2}[s]
            token_copy(d).wait_recv()
            normalize_piece(lax.rem(tp + tps - d, tps))
    pump(1)
    low = nt(normed[...], inner[...]).astype(bf16)
    cols = pl.ds(pl.multiple_of(tp * qc, qc), qc)
    lane2 = lax.broadcasted_iota(jnp.int32, (1, 2 * qc), 1)
    heads = spikes.shape[0]
    padded = jnp.concatenate([spikes[...], jnp.zeros((8 - heads, seq), f32)], axis=0)
    chosen = (
        lax.broadcasted_iota(jnp.int32, (8, qc), 1) // KEY_CHANNELS
        == lax.broadcasted_iota(jnp.int32, (8, qc), 0)
    ).astype(f32)
    spread = lax.dot_general(
        padded, chosen, (((0,), (0,)), ((), ())), precision=highest, preferred_element_type=f32
    )
    for direction in range(2):
        pre = nn(
            low[:, direction * RANK : (direction + 1) * RANK], outer[direction, :, cols]
        ) + bias[direction : direction + 1, cols]
        ld[:, direction * qc : (direction + 1) * qc] = (
            jnp.minimum(pre, 0.0) - jnp.log1p(jnp.exp(-jnp.abs(pre)))
        ) / gate_norm_factor + spread
    in_step(n - 1)
    pump(1)

    pbuf[pl.ds(RIM, seq), :] = nn(normed[...], wbuf[:, :pc]).astype(bf16)

    def halo(side):
        src = pl.ds(seq, RIM) if side == 0 else pl.ds(RIM, RIM)
        dst = pl.ds(0, RIM) if side == 0 else pl.ds(RIM + seq, RIM)
        peer = jnp.minimum(me + 1, n - 1) if side == 0 else jnp.maximum(me - 1, 0)
        return pltpu.make_async_remote_copy(
            src_ref=pbuf.at[src],
            dst_ref=pbuf.at[dst],
            send_sem=halo_send.at[side],
            recv_sem=halo_recv.at[side],
            device_id={"sp": peer},
            device_id_type=MESH,
        )

    @pl.when(me < n - 1)
    def _():
        halo(0).start()

    @pl.when(me > 0)
    def _():
        halo(1).start()

    @pl.when(me == 0)
    def _():
        pbuf[pl.ds(0, RIM), :] = jnp.zeros((RIM, pc), bf16)

    @pl.when(me == n - 1)
    def _():
        pbuf[pl.ds(RIM + seq, RIM), :] = jnp.zeros((RIM, pc), bf16)

    qkv[...] = nn(normed[...], wbuf[:, pc:]).astype(bf16)
    pump(1)

    row_ids = lax.broadcasted_iota(jnp.int32, (BLOCK, BLOCK), 0)
    col_ids = lax.broadcasted_iota(jnp.int32, (BLOCK, BLOCK), 1)
    lower = (col_ids <= row_ids).astype(f32)
    upper = (col_ids >= row_ids).astype(f32)
    first = lax.broadcasted_iota(jnp.int32, (1, qc), 1) < KEY_CHANNELS
    k0 = first.astype(f32)
    k1 = 1.0 - k0
    first2 = lax.rem(lane2, qc) < KEY_CHANNELS
    v0 = (lax.broadcasted_iota(jnp.int32, (1, vc), 1) < DV).astype(f32)
    v1 = 1.0 - v0
    allowed = (
        lax.rem(lax.broadcasted_iota(jnp.int32, (BLOCK, qc), 1), BLOCK)
        <= lax.broadcasted_iota(jnp.int32, (BLOCK, qc), 0)
    )

    for b in range(blocks):
        at = pl.ds(b * BLOCK, BLOCK)
        cum_f = jnp.dot(lower, ld[at, :qc], precision=highest, preferred_element_type=f32)
        cum_b = jnp.dot(upper, ld[at, qc:], precision=highest, preferred_element_type=f32)
        q = qkv[at, :qc].astype(f32) * KEY_CHANNELS ** (-0.5)
        k = qkv[at, qc : 2 * qc].astype(f32)
        v = qkv[at, 2 * qc :]
        vf = v.astype(f32)
        qf = (q * jnp.exp(cum_f)).astype(bf16)
        qb = (q * jnp.exp(cum_b)).astype(bf16)
        kf = k * jnp.exp(-cum_f)
        kb = k * jnp.exp(-cum_b)
        edge_f = cum_f[BLOCK - 1 : BLOCK, :]
        edge_b = cum_b[0:1, :]
        weighted = jnp.concatenate(
            [k * jnp.exp(edge_f - cum_f), k * jnp.exp(edge_b - cum_b)], axis=1
        ).astype(bf16)
        qbuf[at, :qc] = qf
        qbuf[at, qc:] = qb
        edges[b : b + 1, :] = jnp.concatenate([edge_f, edge_b], axis=1)
        scores_f = nt(qf, jnp.concatenate([kf * k0, kf * k1], axis=0).astype(bf16))
        scores_b = nt(qb, jnp.concatenate([kb * k0, kb * k1], axis=0).astype(bf16))
        scores = jnp.where(allowed, scores_f, scores_b).astype(bf16)
        both = jnp.concatenate([vf * v0, vf * v1], axis=0).astype(bf16)
        acc[at, :] = nn(scores, both)
        full = tn(v, weighted)
        upd[b] = jnp.where(first2, full[:DV], full[DV:])
        if b % 2 == 1:
            pump(1)

    total_f = jnp.zeros((DV, qc), f32)
    total_b = jnp.zeros((DV, qc), f32)
    for b in range(blocks):
        total_f = jnp.exp(edges[b : b + 1, :qc]) * total_f + upd[b, :, :qc]
    for b in reversed(range(blocks)):
        total_b = jnp.exp(edges[b : b + 1, qc:]) * total_b + upd[b, :, qc:]
    logs = jnp.sum(edges[...], axis=0, keepdims=True)
    ids = lax.broadcasted_iota(jnp.int32, (RIM, qc), 0)
    for direction, total in ((0, total_f), (1, total_b)):
        msg[direction, pl.ds(0, DV), :] = total.astype(bf16)
        log = logs[:, direction * qc : (direction + 1) * qc]
        hi = log.astype(bf16).astype(f32)
        lo = log - hi
        msg[direction, pl.ds(DV, RIM), :] = jnp.where(
            ids == 0, hi, jnp.where(ids == 1, lo, 0.0)
        ).astype(bf16)

    def state_copy(d):
        peer = lax.rem(me + d, n)
        return pltpu.make_async_remote_copy(
            src_ref=msg.at[jnp.where(peer > me, 0, 1)],
            dst_ref=inbox.at[me],
            send_sem=st_send.at[d - 1],
            recv_sem=st_recv.at[d - 1],
            device_id={"sp": peer},
            device_id_type=MESH,
        )

    def state_landed(source):
        d = lax.rem(me - source + n, n)
        return pltpu.make_async_remote_copy(
            src_ref=msg.at[0],
            dst_ref=inbox.at[source],
            send_sem=st_send.at[d - 1],
            recv_sem=st_recv.at[d - 1],
            device_id={"sp": source},
            device_id_type=MESH,
        )

    for d in range(1, n):
        state_copy(d).start()

    @pl.when(me > 0)
    def _():
        halo(0).wait_recv()

    @pl.when(me < n - 1)
    def _():
        halo(1).wait_recv()

    window = jnp.left_shift(jnp.int32(2), tp)
    half_width = window // 2
    tile = 2 * BLOCK
    offset = (
        lax.broadcasted_iota(jnp.int32, (tile, tile + 2 * RIM), 1)
        - RIM
        - lax.broadcasted_iota(jnp.int32, (tile, tile + 2 * RIM), 0)
    )
    band = ((offset >= -half_width) & (offset < window - half_width)).astype(f32).astype(bf16)
    seq_length = seq * n
    for b in range(seq // tile):
        sums = nn(band, pbuf[pl.ds(b * tile, tile + 2 * RIM), :])
        position = me * seq + b * tile + lax.broadcasted_iota(jnp.int32, (tile, 1), 0)
        low_end = jnp.clip(position - half_width, 0, seq_length - 1)
        high_end = jnp.clip(position - half_width + window - 1, 0, seq_length - 1)
        counted = (high_end - low_end + 1).astype(f32)
        pooled = (sums / counted - pbuf[pl.ds(RIM + b * tile, tile), :].astype(f32)).astype(bf16)
        act[pl.ds(b * tile, tile), :pc] = nn(pooled, gmap[...]).astype(bf16)
    def join(source, state):
        state_landed(source).wait_recv()
        tail = inbox[source, pl.ds(DV, RIM), :].astype(f32)
        log = tail[0:1, :] + tail[1:2, :]
        return jnp.exp(log) * state + inbox[source, pl.ds(0, DV), :].astype(f32)

    state_f = lax.fori_loop(0, me, join, start[0].T)
    state_b = lax.fori_loop(0, n - 1 - me, lambda i, st: join(n - 1 - i, st), start[1].T)
    for b in reversed(range(blocks)):
        before_b[b] = state_b
        state_b = jnp.exp(edges[b : b + 1, qc:]) * state_b + upd[b, :, qc:]
    for b in range(blocks):
        at = pl.ds(b * BLOCK, BLOCK)
        back = before_b[b]
        memory = jnp.concatenate(
            [
                jnp.concatenate([state_f * k0, back * k0], axis=1),
                jnp.concatenate([state_f * k1, back * k1], axis=1),
            ],
            axis=0,
        ).astype(bf16)
        joined = acc[at, :] + nt(qbuf[at, :], memory)
        for h in range(vc // DV):
            o = joined[:, h * DV : (h + 1) * DV]
            scale = lax.rsqrt(jnp.mean(o * o, axis=-1, keepdims=True) + eps_value)
            act[at, pc + h * DV : pc + (h + 1) * DV] = (o * scale).astype(bf16)
        if b + 1 < blocks:
            state_f = jnp.exp(edges[b : b + 1, :qc]) * state_f + upd[b, :, :qc]

    for s in range(pumped, n):
        out_step(s)

    sibling = tp + 1 - 2 * lax.rem(tp, 2)
    across = lax.rem(tp + 2, tps)
    across_sibling = lax.rem(sibling + 2, tps)
    ocols = obuf.shape[2]
    xw = n * ocols // X_CHUNKS

    def product(dest, j):
        piece = pl.ds(pl.multiple_of(dest * m, m), m)
        return nn(act[piece, :], obuf[j])

    def sib_copy(slot, c):
        part = pl.ds(c * xw, xw)
        return pltpu.make_async_remote_copy(
            src_ref=sib_out.at[slot, :, part],
            dst_ref=sib_in.at[slot, :, part],
            send_sem=sib_send.at[slot, c],
            recv_sem=sib_recv.at[slot, c],
            device_id={"tp": sibling},
            device_id_type=MESH,
        )

    def x_copy(c):
        part = pl.ds(c * xw, xw)
        return pltpu.make_async_remote_copy(
            src_ref=x_out.at[:, part],
            dst_ref=x_in.at[:, part],
            send_sem=x_send.at[c],
            recv_sem=x_recv.at[c],
            device_id={"tp": across},
            device_id_type=MESH,
        )

    per = n // X_CHUNKS
    for c in range(X_CHUNKS):
        for j in range(c * per, (c + 1) * per):
            sib_out[0, :, j * ocols : (j + 1) * ocols] = product(across_sibling, j).astype(bf16)
        sib_copy(0, c).start()
    for c in range(X_CHUNKS):
        sums = [product(across, j) for j in range(c * per, (c + 1) * per)]
        sib_copy(0, c).wait_recv()
        for i, j in enumerate(range(c * per, (c + 1) * per)):
            at = pl.ds(j * ocols, ocols)
            x_out[:, at] = (sums[i] + sib_in[0, :, at].astype(f32)).astype(bf16)
        x_copy(c).start()
    for c in range(X_CHUNKS):
        for j in range(c * per, (c + 1) * per):
            sib_out[1, :, j * ocols : (j + 1) * ocols] = product(sibling, j).astype(bf16)
        sib_copy(1, c).start()
    for j in range(n):
        own[:, j * ocols : (j + 1) * ocols] = product(tp, j)
    for c in range(X_CHUNKS):
        sib_copy(1, c).wait_recv()
        x_copy(c).wait_recv()
        at = pl.ds(c * xw, xw)
        result[:, at] = (
            own[:, at] + sib_in[1, :, at].astype(f32) + x_in[:, at].astype(f32)
        ).astype(bf16)

    for d in range(1, tps):
        token_copy(d).wait_send()
    for s in range(n - 1):
        for d in range(2):
            for c in range(IN_CHUNKS):
                in_copy(d, c, s).wait_send()
            for c in range(OUT_CHUNKS):
                out_pair(d, c, s, False).wait_send()

    @pl.when(me < n - 1)
    def _():
        halo(0).wait_send()

    @pl.when(me > 0)
    def _():
        halo(1).wait_send()

    for d in range(1, n):
        state_copy(d).wait_send()
    for c in range(X_CHUNKS):
        sib_copy(0, c).wait_send()
        sib_copy(1, c).wait_send()
        x_copy(c).wait_send()


def one_kernel(
    n,
    tps,
    tokens,
    pooling_input_weight,
    query_matrix,
    key_matrix,
    value_matrix,
    decay_inner_weight,
    decay_outer_weight,
    channel_decay_bias,
    spike_log_decay,
    starting_state,
    pooling_group_map,
    pooling_output_weight,
    attention_output_weight,
):
    m, width = tokens.shape
    seq = m * tps
    pc, qc, vc = (a.shape[1] for a in (pooling_input_weight, query_matrix, value_matrix))
    ocols = pooling_output_weight.shape[1]
    blocks = seq // BLOCK
    f32, bf16 = jnp.float32, jnp.bfloat16
    vmem = pl.BlockSpec(memory_space=pltpu.VMEM)
    hbm = pl.BlockSpec(memory_space=pl.ANY)
    dma = pltpu.SemaphoreType.DMA
    return pl.pallas_call(
        functools.partial(fused, n),
        out_shape=jax.ShapeDtypeStruct((m, n * ocols), bf16),
        in_specs=[hbm] * 5 + [vmem] * 5 + [hbm] * 3,
        out_specs=vmem,
        scratch_shapes=[
            pltpu.VMEM((seq, width), bf16),
            pltpu.VMEM((seq, width), bf16),
            pltpu.VMEM((width, pc + 2 * qc + vc), bf16),
            pltpu.VMEM((n, pc + vc, ocols), bf16),
            pltpu.VMEM((seq + 2 * RIM, pc), bf16),
            pltpu.VMEM((seq, 2 * qc + vc), bf16),
            pltpu.VMEM((seq, 2 * qc), f32),
            pltpu.VMEM((seq, 2 * qc), bf16),
            pltpu.VMEM((blocks, DV, 2 * qc), f32),
            pltpu.VMEM((blocks, 2 * qc), f32),
            pltpu.VMEM((blocks, DV, qc), f32),
            pltpu.VMEM((seq, vc), f32),
            pltpu.VMEM((seq, pc + vc), bf16),
            pltpu.VMEM((2, DV + RIM, qc), bf16),
            pltpu.VMEM((n, DV + RIM, qc), bf16),
            pltpu.VMEM((pc, pc), bf16),
            pltpu.VMEM((2, m, n * ocols), bf16),
            pltpu.VMEM((2, m, n * ocols), bf16),
            pltpu.VMEM((m, n * ocols), bf16),
            pltpu.VMEM((m, n * ocols), bf16),
            pltpu.VMEM((m, n * ocols), f32),
            dma((8,)),
            dma((tps - 1,)),
            dma((tps - 1,)),
            dma((2, IN_CHUNKS, n - 1)),
            dma((2, IN_CHUNKS, n - 1)),
            dma((2, OUT_CHUNKS, n - 1)),
            dma((2, OUT_CHUNKS, n - 1)),
            dma((2,)),
            dma((2,)),
            dma((n - 1,)),
            dma((n - 1,)),
            dma((2, X_CHUNKS)),
            dma((2, X_CHUNKS)),
            dma((X_CHUNKS,)),
            dma((X_CHUNKS,)),
        ],
        compiler_params=pltpu.CompilerParams(
            collective_id=0, has_side_effects=True, vmem_limit_bytes=60 * 2**20
        ),
    )(
        tokens,
        pooling_input_weight,
        query_matrix,
        key_matrix,
        value_matrix,
        decay_inner_weight.T,
        decay_outer_weight,
        channel_decay_bias,
        spike_log_decay,
        starting_state.reshape(2, qc, DV),
        pooling_group_map,
        pooling_output_weight,
        attention_output_weight,
    )


def solution(mesh):
    in_specs = (
        P(("sp", "tp"), None),
        P("sp", "tp"),
        P("sp", "tp"),
        P("sp", "tp"),
        P("sp", "tp"),
        P(),
        P(),
        P(),
        P("tp", "sp"),
        P(None, "tp", None, None),
        P(),
        P("tp", "sp"),
        P("tp", "sp"),
    )
    out_specs = P(("sp", "tp"), None)
    n, tps = mesh.shape["sp"], mesh.shape["tp"]
    fits = n % X_CHUNKS == 0 and n <= 16 and tps == 4
    local = functools.partial(one_kernel, n, tps) if fits else shards
    return jax.shard_map(local, mesh=mesh, in_specs=in_specs, out_specs=out_specs, check_vma=False)
```

profile of v0, /device:TPU:0, one launch (start us, length us, event | category | flops | bytes accessed | tf_op | source)
XLA Modules:
  0.0 88.3 jit_solution(4316332651402961692)
XLA Ops:
  0.0 86.4 %shard_map.127 = bf16[128,2048]{1,0:T(8,128)(2,1)} custom-call(bf16[128,2048]{1,0:T(8,128)(2,1)} %tokens.1, bf16[256,256]{1,0:T(8,128)(2,1)} %w_pool.1, bf16[256,128]{1,0:T(8,128)(2,1)} %w_query.1, bf16[256,128]{1,0:T(8,128)(2,1)} %w_key.1, bf16[256,256]{1,0:T(8,128)(2,1)} %w_value.1, bf16[64,2048]{1,0:T(8,128)(2,1)} %bitcast.2, bf16[2,32,512]{2,1,0:T(8,128)(2,1)} %outer.1, ...), custom_call_target="tpu_custom_call" | custom-call | tf_op jit(solution)/shard_map/pallas_call | solution.py:779
  86.4 1.9 %copy.15 = bf16[128,2048]{1,0:T(8,128)(2,1)} copy(bf16[128,2048]{1,0:T(8,128)(2,1)} %shard_map.127) | data formatting | bytes 1048576
where the time goes:
time: 88.4 us; the launch traced here: 88.3 us
  Pallas kernels  86.4 us (98%)
  local copies, waits for them, and re-layouts  1.88 us (2%)
    pallas_call x1, Pallas kernels, one_kernel(): pl.pallas_call(functools.partial(fused, n), out_shape=jax.ShapeDtypeStruc...  86.4 us
    unnamed x1, local copies, waits for them, and re-layouts  1.88 us

commit v1 on v0

--- a/solution.py
+++ b/solution.py
@@ -234,11 +234,10 @@
 
 
 MESH = pl.DeviceIdType.MESH
-IN_CHUNKS = 3
-OUT_CHUNKS = 4
+CHUNKS = 4
+TOK_CHUNKS = 4
 RIM = 16
-X_CHUNKS = 4
-EARLY = (0, 0, 1, 1, 1, 1, 1)
+QKV, POOL, OUT = range(3)
 
 
 def nt(a, b):
@@ -271,7 +270,8 @@
     result,
     xraw,
     normed,
-    wbuf,
+    wqkv,
+    wpl,
     obuf,
     pbuf,
     qkv,
@@ -287,16 +287,15 @@
     gmap,
     sib_out,
     sib_in,
+    x_part,
     x_out,
     x_in,
     own,
     local_sem,
     tok_send,
     tok_recv,
-    in_send,
-    in_recv,
-    out_send,
-    out_recv,
+    ring_send,
+    ring_recv,
     halo_send,
     halo_recv,
     st_send,
@@ -313,7 +312,7 @@
     seq = normed.shape[0]
     rows = w_pool.shape[0]
     pc, qc, vc = w_pool.shape[1], w_query.shape[1], w_value.shape[1]
-    width = pc + 2 * qc + vc
+    ocols = obuf.shape[2]
     blocks = seq // BLOCK
     half = n // 2
     f32, bf16 = jnp.float32, jnp.bfloat16
@@ -326,6 +325,11 @@
         return jnp.where(p < half, 2 * p, 2 * (n - 1 - p) + 1)
 
     nexts = (at_pos(pos + 1), at_pos(pos - 1))
+    origins = {k: at_pos(pos + k) for k in range(-half, half + 1)}
+
+    sibling = tp + 1 - 2 * lax.rem(tp, 2)
+    across = lax.rem(tp + 2, tps)
+    across_sibling = lax.rem(sibling + 2, tps)
 
     locals_ = []
 
@@ -336,19 +340,19 @@
         return copy
 
     my_rows = pl.ds(pl.multiple_of(me * rows, rows), rows)
+    my_tok = pl.ds(pl.multiple_of(tp * m, m), m)
     w_copies = [
-        local(w_pool, wbuf.at[my_rows, pl.ds(0, pc)]),
-        local(w_query, wbuf.at[my_rows, pl.ds(pc, qc)]),
-        local(w_key, wbuf.at[my_rows, pl.ds(pc + qc, qc)]),
-        local(w_value, wbuf.at[my_rows, pl.ds(pc + 2 * qc, vc)]),
+        local(w_query, wqkv.at[my_rows, pl.ds(0, qc)]),
+        local(w_key, wqkv.at[my_rows, pl.ds(qc, qc)]),
+        local(w_value, wqkv.at[my_rows, pl.ds(2 * qc, vc)]),
     ]
-    o_copies = [
+    t_copy = local(tokens, xraw.at[my_tok])
+    late_copies = [
+        local(w_pool, wpl.at[my_rows]),
         local(w_pool_out, obuf.at[me, pl.ds(0, pc)]),
         local(w_att_out, obuf.at[me, pl.ds(pc, vc)]),
+        local(group_map.at[tp], gmap),
     ]
-    my_tok = pl.ds(pl.multiple_of(tp * m, m), m)
-    t_copy = local(tokens, xraw.at[my_tok])
-    g_copy = local(group_map.at[tp], gmap)
 
     barrier = pltpu.get_barrier_semaphore()
     for d in range(1, n):
@@ -361,111 +365,98 @@
         )
     pl.semaphore_wait(barrier, n - 1 + tps - 1)
 
-    def token_copy(d):
-        return pltpu.make_async_remote_copy(
-            src_ref=tokens,
-            dst_ref=xraw.at[my_tok],
-            send_sem=tok_send.at[d - 1],
-            recv_sem=tok_recv.at[d - 1],
-            device_id={"tp": lax.rem(tp + d, tps)},
-            device_id_type=MESH,
-        )
-
-    def in_copy(d, c, s):
-        origin = at_pos(pos - s if d == 0 else pos + s)
-        step = width // (2 * IN_CHUNKS)
-        part = wbuf.at[
-            pl.ds(pl.multiple_of(origin * rows, rows), rows),
-            pl.ds((d * IN_CHUNKS + c) * step, step),
-        ]
+    def hops_of(d, c):
+        return half if (c < CHUNKS // 2) == (d == 0) else half - 1
+
+    def ring_copy(group, d, c, s, landed):
+        shift = s + 1 if landed else s
+        origin = origins[-shift if d == 0 else shift]
+        if group == OUT:
+            step = (pc + vc) // CHUNKS
+            part = obuf.at[origin, pl.ds(c * step, step)]
+        else:
+            step = rows // CHUNKS
+            at = pl.ds(pl.multiple_of(origin * rows + c * step, step), step)
+            part = wqkv.at[at] if group == QKV else wpl.at[at]
         return pltpu.make_async_remote_copy(
             src_ref=part,
             dst_ref=part,
-            send_sem=in_send.at[d, c, s],
-            recv_sem=in_recv.at[d, c, s],
+            send_sem=ring_send.at[group, d, c, s],
+            recv_sem=ring_recv.at[group, d, c, s],
             device_id={"sp": nexts[d]},
             device_id_type=MESH,
         )
 
-    def in_landed(d, c, s):
-        origin = at_pos(pos - s - 1 if d == 0 else pos + s + 1)
-        step = width // (2 * IN_CHUNKS)
-        part = wbuf.at[
-            pl.ds(pl.multiple_of(origin * rows, rows), rows),
-            pl.ds((d * IN_CHUNKS + c) * step, step),
-        ]
+    def ring_event(group, s, i):
+        for d in range(2):
+            c = i if d == 0 else (i + CHUNKS // 2) % CHUNKS
+            hops = hops_of(d, c)
+            if 0 < s <= hops:
+                ring_copy(group, d, c, s - 1, True).wait_recv()
+            if s < hops:
+                ring_copy(group, d, c, s, False).start()
+
+    order = event_order(half)
+    done = 0
+
+    def pump(count=1):
+        nonlocal done
+        for event in order[done : done + count]:
+            ring_event(*event)
+        done = min(done + count, len(order))
+
+    def pump_to(event):
+        pump(order.index(event) + 1 - done)
+
+    def token_copy(kind, c=0):
+        step = m // TOK_CHUNKS
+        if kind == 0:
+            slot, part, peer = 0, my_tok, sibling
+        elif kind == 1:
+            slot, peer = 1 + c, across
+            part = pl.ds(pl.multiple_of(tp * m + c * step, step), step)
+        else:
+            slot, peer = 1 + TOK_CHUNKS + c, sibling
+            part = pl.ds(pl.multiple_of(across * m + c * step, step), step)
         return pltpu.make_async_remote_copy(
-            src_ref=part,
-            dst_ref=part,
-            send_sem=in_send.at[d, c, s],
-            recv_sem=in_recv.at[d, c, s],
-            device_id={"sp": nexts[d]},
+            src_ref=xraw.at[part],
+            dst_ref=xraw.at[part],
+            send_sem=tok_send.at[slot],
+            recv_sem=tok_recv.at[slot],
+            device_id={"tp": peer},
             device_id_type=MESH,
         )
 
-    def out_pair(d, c, s, landed):
-        shift = s + 1 if landed else s
-        origin = at_pos(pos - shift if d == 0 else pos + shift)
-        step = (pc + vc) // (2 * OUT_CHUNKS)
-        part = obuf.at[origin, pl.ds((d * OUT_CHUNKS + c) * step, step)]
-        return pltpu.make_async_remote_copy(
-            src_ref=part,
-            dst_ref=part,
-            send_sem=out_send.at[d, c, s],
-            recv_sem=out_recv.at[d, c, s],
-            device_id={"sp": nexts[d]},
-            device_id_type=MESH,
-        )
-
-    def in_step(s):
-        for c in range(IN_CHUNKS):
-            for d in range(2):
-                if s > 0:
-                    in_landed(d, c, s - 1).wait_recv()
-                if s < n - 1:
-                    in_copy(d, c, s).start()
-
-    def out_step(s):
-        for c in range(OUT_CHUNKS):
-            for d in range(2):
-                if s > 0:
-                    out_pair(d, c, s - 1, True).wait_recv()
-                if s < n - 1:
-                    out_pair(d, c, s, False).start()
-
-    def normalize_piece(source):
-        piece = pl.ds(pl.multiple_of(source * m, m), m)
+    def normalize_rows(source, c, count):
+        piece = pl.ds(pl.multiple_of(source * m + c * count, count), count)
         floats = xraw[piece, :].astype(f32)
         scale = lax.rsqrt(jnp.mean(floats * floats, axis=-1, keepdims=True) + eps_value)
         normed[piece, :] = (floats * scale).astype(bf16)
 
-    pumped = 0
-
-    def pump(count):
-        nonlocal pumped
-        for s in range(pumped, min(pumped + count, n - 1)):
-            out_step(s)
-            pumped = s + 1
-
+    t_copy.wait()
+    for c in range(TOK_CHUNKS):
+        token_copy(1, c).start()
+    token_copy(0).start()
     for copy in w_copies:
         copy.wait()
-    in_step(0)
-    for d in (2, 1, 3):
-        token_copy(d).start()
-    for copy in o_copies:
+    pump(CHUNKS)
+    for copy in late_copies:
         copy.wait()
-    t_copy.wait()
-    g_copy.wait()
-    in_step(1)
-    normalize_piece(tp)
-    for s in range(2, n - 1):
-        in_step(s)
-        pump(EARLY[s] if s < len(EARLY) else 0)
-        if s in (3, 4, 5):
-            d = {3: 1, 4: 3, 5: 2}[s]
-            token_copy(d).wait_recv()
-            normalize_piece(lax.rem(tp + tps - d, tps))
+    normalize_rows(tp, 0, m)
+    token_copy(0).wait_recv()
+    normalize_rows(sibling, 0, m)
     pump(1)
+    for c in range(TOK_CHUNKS):
+        token_copy(1, c).wait_recv()
+        token_copy(2, c).start()
+        normalize_rows(across, c, m // TOK_CHUNKS)
+        if c > 0:
+            token_copy(2, c - 1).wait_recv()
+            normalize_rows(across_sibling, c - 1, m // TOK_CHUNKS)
+        pump(2)
+    token_copy(2, TOK_CHUNKS - 1).wait_recv()
+    normalize_rows(across_sibling, TOK_CHUNKS - 1, m // TOK_CHUNKS)
+
     low = nt(normed[...], inner[...]).astype(bf16)
     cols = pl.ds(pl.multiple_of(tp * qc, qc), qc)
     lane2 = lax.broadcasted_iota(jnp.int32, (1, 2 * qc), 1)
@@ -485,41 +476,9 @@
         ld[:, direction * qc : (direction + 1) * qc] = (
             jnp.minimum(pre, 0.0) - jnp.log1p(jnp.exp(-jnp.abs(pre)))
         ) / gate_norm_factor + spread
-    in_step(n - 1)
-    pump(1)
-
-    pbuf[pl.ds(RIM, seq), :] = nn(normed[...], wbuf[:, :pc]).astype(bf16)
-
-    def halo(side):
-        src = pl.ds(seq, RIM) if side == 0 else pl.ds(RIM, RIM)
-        dst = pl.ds(0, RIM) if side == 0 else pl.ds(RIM + seq, RIM)
-        peer = jnp.minimum(me + 1, n - 1) if side == 0 else jnp.maximum(me - 1, 0)
-        return pltpu.make_async_remote_copy(
-            src_ref=pbuf.at[src],
-            dst_ref=pbuf.at[dst],
-            send_sem=halo_send.at[side],
-            recv_sem=halo_recv.at[side],
-            device_id={"sp": peer},
-            device_id_type=MESH,
-        )
-
-    @pl.when(me < n - 1)
-    def _():
-        halo(0).start()
-
-    @pl.when(me > 0)
-    def _():
-        halo(1).start()
-
-    @pl.when(me == 0)
-    def _():
-        pbuf[pl.ds(0, RIM), :] = jnp.zeros((RIM, pc), bf16)
-
-    @pl.when(me == n - 1)
-    def _():
-        pbuf[pl.ds(RIM + seq, RIM), :] = jnp.zeros((RIM, pc), bf16)
-
-    qkv[...] = nn(normed[...], wbuf[:, pc:]).astype(bf16)
+
+    pump_to((QKV, half, CHUNKS // 2 - 1))
+    qkv[...] = nn(normed[...], wqkv[...]).astype(bf16)
     pump(1)
 
     row_ids = lax.broadcasted_iota(jnp.int32, (BLOCK, BLOCK), 0)
@@ -564,7 +523,7 @@
         acc[at, :] = nn(scores, both)
         full = tn(v, weighted)
         upd[b] = jnp.where(first2, full[:DV], full[DV:])
-        if b % 2 == 1:
+        if b % 4 == 3:
             pump(1)
 
     total_f = jnp.zeros((DV, qc), f32)
@@ -609,32 +568,40 @@
     for d in range(1, n):
         state_copy(d).start()
 
+    pump_to((POOL, half, CHUNKS // 2 - 1))
+    pbuf[pl.ds(RIM, seq), :] = nn(normed[...], wpl[...]).astype(bf16)
+
+    def halo(side):
+        src = pl.ds(seq, RIM) if side == 0 else pl.ds(RIM, RIM)
+        dst = pl.ds(0, RIM) if side == 0 else pl.ds(RIM + seq, RIM)
+        peer = jnp.minimum(me + 1, n - 1) if side == 0 else jnp.maximum(me - 1, 0)
+        return pltpu.make_async_remote_copy(
+            src_ref=pbuf.at[src],
+            dst_ref=pbuf.at[dst],
+            send_sem=halo_send.at[side],
+            recv_sem=halo_recv.at[side],
+            device_id={"sp": peer},
+            device_id_type=MESH,
+        )
+
+    @pl.when(me < n - 1)
+    def _():
+        halo(0).start()
+
     @pl.when(me > 0)
     def _():
-        halo(0).wait_recv()
-
-    @pl.when(me < n - 1)
+        halo(1).start()
+
+    @pl.when(me == 0)
     def _():
-        halo(1).wait_recv()
-
-    window = jnp.left_shift(jnp.int32(2), tp)
-    half_width = window // 2
-    tile = 2 * BLOCK
-    offset = (
-        lax.broadcasted_iota(jnp.int32, (tile, tile + 2 * RIM), 1)
-        - RIM
-        - lax.broadcasted_iota(jnp.int32, (tile, tile + 2 * RIM), 0)
-    )
-    band = ((offset >= -half_width) & (offset < window - half_width)).astype(f32).astype(bf16)
-    seq_length = seq * n
-    for b in range(seq // tile):
-        sums = nn(band, pbuf[pl.ds(b * tile, tile + 2 * RIM), :])
-        position = me * seq + b * tile + lax.broadcasted_iota(jnp.int32, (tile, 1), 0)
-        low_end = jnp.clip(position - half_width, 0, seq_length - 1)
-        high_end = jnp.clip(position - half_width + window - 1, 0, seq_length - 1)
-        counted = (high_end - low_end + 1).astype(f32)
-        pooled = (sums / counted - pbuf[pl.ds(RIM + b * tile, tile), :].astype(f32)).astype(bf16)
-        act[pl.ds(b * tile, tile), :pc] = nn(pooled, gmap[...]).astype(bf16)
+        pbuf[pl.ds(0, RIM), :] = jnp.zeros((RIM, pc), bf16)
+
+    @pl.when(me == n - 1)
+    def _():
+        pbuf[pl.ds(RIM + seq, RIM), :] = jnp.zeros((RIM, pc), bf16)
+
+    pump(1)
+
     def join(source, state):
         state_landed(source).wait_recv()
         tail = inbox[source, pl.ds(DV, RIM), :].astype(f32)
@@ -663,76 +630,109 @@
             act[at, pc + h * DV : pc + (h + 1) * DV] = (o * scale).astype(bf16)
         if b + 1 < blocks:
             state_f = jnp.exp(edges[b : b + 1, :qc]) * state_f + upd[b, :, :qc]
-
-    for s in range(pumped, n):
-        out_step(s)
-
-    sibling = tp + 1 - 2 * lax.rem(tp, 2)
-    across = lax.rem(tp + 2, tps)
-    across_sibling = lax.rem(sibling + 2, tps)
-    ocols = obuf.shape[2]
-    xw = n * ocols // X_CHUNKS
-
-    def product(dest, j):
-        piece = pl.ds(pl.multiple_of(dest * m, m), m)
-        return nn(act[piece, :], obuf[j])
-
-    def sib_copy(slot, c):
-        part = pl.ds(c * xw, xw)
+    pump(1)
+
+    @pl.when(me > 0)
+    def _():
+        halo(0).wait_recv()
+
+    @pl.when(me < n - 1)
+    def _():
+        halo(1).wait_recv()
+
+    window = jnp.left_shift(jnp.int32(2), tp)
+    half_width = window // 2
+    tile = 2 * BLOCK
+    offset = (
+        lax.broadcasted_iota(jnp.int32, (tile, tile + 2 * RIM), 1)
+        - RIM
+        - lax.broadcasted_iota(jnp.int32, (tile, tile + 2 * RIM), 0)
+    )
+    band = ((offset >= -half_width) & (offset < window - half_width)).astype(f32).astype(bf16)
+    seq_length = seq * n
+    for b in range(seq // tile):
+        sums = nn(band, pbuf[pl.ds(b * tile, tile + 2 * RIM), :])
+        position = me * seq + b * tile + lax.broadcasted_iota(jnp.int32, (tile, 1), 0)
+        low_end = jnp.clip(position - half_width, 0, seq_length - 1)
+        high_end = jnp.clip(position - half_width + window - 1, 0, seq_length - 1)
+        counted = (high_end - low_end + 1).astype(f32)
+        pooled = (sums / counted - pbuf[pl.ds(RIM + b * tile, tile), :].astype(f32)).astype(bf16)
+        act[pl.ds(b * tile, tile), :pc] = nn(pooled, gmap[...]).astype(bf16)
+
+    block_at = [0]
+    for k in range(1, half):
+        block_at += [-k, k]
+    block_at.append(half)
+
+    def rows_of(dest):
+        return pl.ds(pl.multiple_of(dest * m, m), m)
+
+    def sib_copy(i):
         return pltpu.make_async_remote_copy(
-            src_ref=sib_out.at[slot, :, part],
-            dst_ref=sib_in.at[slot, :, part],
-            send_sem=sib_send.at[slot, c],
-            recv_sem=sib_recv.at[slot, c],
+            src_ref=sib_out.at[i],
+            dst_ref=sib_in.at[i],
+            send_sem=sib_send.at[i],
+            recv_sem=sib_recv.at[i],
             device_id={"tp": sibling},
             device_id_type=MESH,
         )
 
-    def x_copy(c):
-        part = pl.ds(c * xw, xw)
+    def x_copy(i):
         return pltpu.make_async_remote_copy(
-            src_ref=x_out.at[:, part],
-            dst_ref=x_in.at[:, part],
-            send_sem=x_send.at[c],
-            recv_sem=x_recv.at[c],
+            src_ref=x_out.at[i],
+            dst_ref=x_in.at[i],
+            send_sem=x_send.at[i],
+            recv_sem=x_recv.at[i],
             device_id={"tp": across},
             device_id_type=MESH,
         )
 
-    per = n // X_CHUNKS
-    for c in range(X_CHUNKS):
-        for j in range(c * per, (c + 1) * per):
-            sib_out[0, :, j * ocols : (j + 1) * ocols] = product(across_sibling, j).astype(bf16)
-        sib_copy(0, c).start()
-    for c in range(X_CHUNKS):
-        sums = [product(across, j) for j in range(c * per, (c + 1) * per)]
-        sib_copy(0, c).wait_recv()
-        for i, j in enumerate(range(c * per, (c + 1) * per)):
-            at = pl.ds(j * ocols, ocols)
-            x_out[:, at] = (sums[i] + sib_in[0, :, at].astype(f32)).astype(bf16)
-        x_copy(c).start()
-    for c in range(X_CHUNKS):
-        for j in range(c * per, (c + 1) * per):
-            sib_out[1, :, j * ocols : (j + 1) * ocols] = product(sibling, j).astype(bf16)
-        sib_copy(1, c).start()
-    for j in range(n):
-        own[:, j * ocols : (j + 1) * ocols] = product(tp, j)
-    for c in range(X_CHUNKS):
-        sib_copy(1, c).wait_recv()
-        x_copy(c).wait_recv()
-        at = pl.ds(c * xw, xw)
+    def produce(i):
+        weights = obuf[origins[block_at[i]]]
+        sib_out[i, pl.ds(0, m)] = nn(act[rows_of(across_sibling), :], weights).astype(bf16)
+        sib_out[i, pl.ds(m, m)] = nn(act[rows_of(sibling), :], weights).astype(bf16)
+        sib_copy(i).start()
+        x_part[i] = nn(act[rows_of(across), :], weights)
+        own[i] = nn(act[rows_of(tp), :], weights)
+
+    def cross(i):
+        sib_copy(i).wait_recv()
+        x_out[i] = (x_part[i] + sib_in[i, pl.ds(0, m)].astype(f32)).astype(bf16)
+        x_copy(i).start()
+
+    def finish(i):
+        x_copy(i).wait_recv()
+        at = pl.ds(pl.multiple_of(origins[block_at[i]] * ocols, ocols), ocols)
         result[:, at] = (
-            own[:, at] + sib_in[1, :, at].astype(f32) + x_in[:, at].astype(f32)
+            own[i] + sib_in[i, pl.ds(m, m)].astype(f32) + x_in[i].astype(f32)
         ).astype(bf16)
 
-    for d in range(1, tps):
-        token_copy(d).wait_send()
-    for s in range(n - 1):
+    produce(0)
+    for s in range(1, half):
+        pump_to((OUT, s, CHUNKS - 1))
+        produce(2 * s - 1)
+        cross(2 * s - 2)
+        produce(2 * s)
+        cross(2 * s - 1)
+        if s > 1:
+            finish(2 * s - 4)
+            finish(2 * s - 3)
+    pump(len(order))
+    produce(n - 1)
+    cross(n - 2)
+    cross(n - 1)
+    for i in range(n - 4, n):
+        finish(i)
+
+    token_copy(0).wait_send()
+    for c in range(TOK_CHUNKS):
+        token_copy(1, c).wait_send()
+        token_copy(2, c).wait_send()
+    for group in range(3):
         for d in range(2):
-            for c in range(IN_CHUNKS):
-                in_copy(d, c, s).wait_send()
-            for c in range(OUT_CHUNKS):
-                out_pair(d, c, s, False).wait_send()
+            for c in range(CHUNKS):
+                for s in range(hops_of(d, c)):
+                    ring_copy(group, d, c, s, False).wait_send()
 
     @pl.when(me < n - 1)
     def _():
@@ -744,10 +744,30 @@
 
     for d in range(1, n):
         state_copy(d).wait_send()
-    for c in range(X_CHUNKS):
-        sib_copy(0, c).wait_send()
-        sib_copy(1, c).wait_send()
-        x_copy(c).wait_send()
+    for i in range(n):
+        sib_copy(i).wait_send()
+        x_copy(i).wait_send()
+
+
+def event_order(half):
+    lead, rest = range(CHUNKS // 2), range(CHUNKS // 2, CHUNKS)
+    events = [(QKV, s, i) for s in range(half - 1) for i in range(CHUNKS)]
+    events += [(QKV, half - 1, i) for i in lead]
+    events += [(POOL, 0, i) for i in range(CHUNKS)]
+    events += [(QKV, half - 1, i) for i in rest]
+    events += [(QKV, half, i) for i in lead]
+    events += [(OUT, 0, 0)]
+    for s in range(1, half - 1):
+        events += [(POOL, s, i) for i in range(CHUNKS)] + [(OUT, 0, s)] * (s < CHUNKS)
+    events += [(POOL, half - 1, i) for i in lead]
+    events += [(OUT, 0, i) for i in range(half - 1, CHUNKS)]
+    events += [(POOL, half - 1, i) for i in rest]
+    events += [(POOL, half, i) for i in lead]
+    for s in range(1, half - 1):
+        events += [(OUT, s, i) for i in range(CHUNKS)]
+    events += [(OUT, half - 1, i) for i in range(CHUNKS)]
+    events += [(OUT, half, i) for i in lead]
+    return events
 
 
 def one_kernel(
@@ -784,7 +804,8 @@
         scratch_shapes=[
             pltpu.VMEM((seq, width), bf16),
             pltpu.VMEM((seq, width), bf16),
-            pltpu.VMEM((width, pc + 2 * qc + vc), bf16),
+            pltpu.VMEM((width, 2 * qc + vc), bf16),
+            pltpu.VMEM((width, pc), bf16),
             pltpu.VMEM((n, pc + vc, ocols), bf16),
             pltpu.VMEM((seq + 2 * RIM, pc), bf16),
             pltpu.VMEM((seq, 2 * qc + vc), bf16),
@@ -798,26 +819,25 @@
             pltpu.VMEM((2, DV + RIM, qc), bf16),
             pltpu.VMEM((n, DV + RIM, qc), bf16),
             pltpu.VMEM((pc, pc), bf16),
-            pltpu.VMEM((2, m, n * ocols), bf16),
-            pltpu.VMEM((2, m, n * ocols), bf16),
-            pltpu.VMEM((m, n * ocols), bf16),
-            pltpu.VMEM((m, n * ocols), bf16),
-            pltpu.VMEM((m, n * ocols), f32),
+            pltpu.VMEM((n, 2 * m, ocols), bf16),
+            pltpu.VMEM((n, 2 * m, ocols), bf16),
+            pltpu.VMEM((n, m, ocols), f32),
+            pltpu.VMEM((n, m, ocols), bf16),
+            pltpu.VMEM((n, m, ocols), bf16),
+            pltpu.VMEM((n, m, ocols), f32),
             dma((8,)),
-            dma((tps - 1,)),
-            dma((tps - 1,)),
-            dma((2, IN_CHUNKS, n - 1)),
-            dma((2, IN_CHUNKS, n - 1)),
-            dma((2, OUT_CHUNKS, n - 1)),
-            dma((2, OUT_CHUNKS, n - 1)),
+            dma((1 + 2 * TOK_CHUNKS,)),
+            dma((1 + 2 * TOK_CHUNKS,)),
+            dma((3, 2, CHUNKS, n // 2)),
+            dma((3, 2, CHUNKS, n // 2)),
             dma((2,)),
             dma((2,)),
             dma((n - 1,)),
             dma((n - 1,)),
-            dma((2, X_CHUNKS)),
-            dma((2, X_CHUNKS)),
-            dma((X_CHUNKS,)),
-            dma((X_CHUNKS,)),
+            dma((n,)),
+            dma((n,)),
+            dma((n,)),
+            dma((n,)),
         ],
         compiler_params=pltpu.CompilerParams(
             collective_id=0, has_side_effects=True, vmem_limit_bytes=60 * 2**20
@@ -857,6 +877,6 @@
     )
     out_specs = P(("sp", "tp"), None)
     n, tps = mesh.shape["sp"], mesh.shape["tp"]
-    fits = n % X_CHUNKS == 0 and n <= 16 and tps == 4
+    fits = n % 4 == 0 and n <= 16 and tps == 4
     local = functools.partial(one_kernel, n, tps) if fits else shards
     return jax.shard_map(local, mesh=mesh, in_specs=in_specs, out_specs=out_specs, check_vma=False)

time: 88.4 us -> 79.4 us (0.90)
  Pallas kernels: 86.4 us -> 77.3 us
    pallas_call x1, Pallas kernels: 86.4 us -> 77.3 us  [one_kernel(): pl.pallas_call(functools.partial(fused, n), out_shape=jax.ShapeDtypeStruc...]
where the time goes in v1:
time: 79.4 us; the launch traced here: 79.2 us
  Pallas kernels  77.3 us (97%)
  local copies, waits for them, and re-layouts  1.88 us (2%)
    pallas_call x1, Pallas kernels, one_kernel(): pl.pallas_call(functools.partial(fused, n), out_shape=jax.ShapeDtypeStruc...  77.3 us
    unnamed x1, local copies, waits for them, and re-layouts  1.88 us

profile of v1, /device:TPU:0, one launch (start us, length us, event | category | flops | bytes accessed | tf_op | source)
XLA Modules:
  0.0 79.2 jit_solution(1966480587399697019)
XLA Ops:
  0.0 77.3 %shard_map.127 = bf16[128,2048]{1,0:T(8,128)(2,1)} custom-call(bf16[128,2048]{1,0:T(8,128)(2,1)} %tokens.1, bf16[256,256]{1,0:T(8,128)(2,1)} %w_pool.1, bf16[256,128]{1,0:T(8,128)(2,1)} %w_query.1, bf16[256,128]{1,0:T(8,128)(2,1)} %w_key.1, bf16[256,256]{1,0:T(8,128)(2,1)} %w_value.1, bf16[64,2048]{1,0:T(8,128)(2,1)} %bitcast.2, bf16[2,32,512]{2,1,0:T(8,128)(2,1)} %outer.1, ...), custom_call_target="tpu_custom_call" | custom-call | tf_op jit(solution)/shard_map/pallas_call | solution.py:799
  77.3 1.9 %copy.15 = bf16[128,2048]{1,0:T(8,128)(2,1)} copy(bf16[128,2048]{1,0:T(8,128)(2,1)} %shard_map.127) | data formatting | bytes 1048576

commit v2 on v1

--- a/solution.py
+++ b/solution.py
@@ -238,6 +238,7 @@
 TOK_CHUNKS = 4
 RIM = 16
 QKV, POOL, OUT = range(3)
+PUMPS = (3, 4)
 
 
 def nt(a, b):
@@ -259,15 +260,20 @@
     w_query,
     w_key,
     w_value,
+    inner_in,
+    outer_in,
+    bias_in,
+    spikes_in,
+    start_in,
+    group_map,
+    w_pool_out,
+    w_att_out,
+    result,
     inner,
     outer,
     bias,
     spikes,
     start,
-    group_map,
-    w_pool_out,
-    w_att_out,
-    result,
     xraw,
     normed,
     wqkv,
@@ -282,8 +288,14 @@
     before_b,
     acc,
     act,
+    total,
+    pair_out,
+    pair_in,
     msg,
     inbox,
+    back_out,
+    back_in,
+    entry,
     gmap,
     sib_out,
     sib_in,
@@ -298,6 +310,8 @@
     ring_recv,
     halo_send,
     halo_recv,
+    pair_send,
+    pair_recv,
     st_send,
     st_recv,
     sib_send,
@@ -339,6 +353,12 @@
         locals_.append(copy)
         return copy
 
+    barrier = pltpu.get_barrier_semaphore()
+    for peer in nexts:
+        pl.semaphore_signal(barrier, inc=1, device_id={"sp": peer}, device_id_type=MESH)
+    for peer in (sibling, across):
+        pl.semaphore_signal(barrier, inc=1, device_id={"tp": peer}, device_id_type=MESH)
+
     my_rows = pl.ds(pl.multiple_of(me * rows, rows), rows)
     my_tok = pl.ds(pl.multiple_of(tp * m, m), m)
     w_copies = [
@@ -352,18 +372,13 @@
         local(w_pool_out, obuf.at[me, pl.ds(0, pc)]),
         local(w_att_out, obuf.at[me, pl.ds(pc, vc)]),
         local(group_map.at[tp], gmap),
+        local(inner_in, inner),
+        local(outer_in, outer),
+        local(bias_in, bias),
+        local(spikes_in, spikes),
+        local(start_in, start),
     ]
-
-    barrier = pltpu.get_barrier_semaphore()
-    for d in range(1, n):
-        pl.semaphore_signal(
-            barrier, inc=1, device_id={"sp": lax.rem(me + d, n)}, device_id_type=MESH
-        )
-    for d in range(1, tps):
-        pl.semaphore_signal(
-            barrier, inc=1, device_id={"tp": lax.rem(tp + d, tps)}, device_id_type=MESH
-        )
-    pl.semaphore_wait(barrier, n - 1 + tps - 1)
+    pl.semaphore_wait(barrier, 4)
 
     def hops_of(d, c):
         return half if (c < CHUNKS // 2) == (d == 0) else half - 1
@@ -533,40 +548,102 @@
     for b in reversed(range(blocks)):
         total_b = jnp.exp(edges[b : b + 1, qc:]) * total_b + upd[b, :, qc:]
     logs = jnp.sum(edges[...], axis=0, keepdims=True)
+    log_f, log_b = logs[:, :qc], logs[:, qc:]
+    total[0] = total_f
+    total[1] = total_b
+    plane, planes = me // 2, n // 2
+    hd = DV // 2
+    my_half = pl.ds(pl.multiple_of(odd * hd, hd), hd)
+    other_half = pl.ds(pl.multiple_of((1 - odd) * hd, hd), hd)
     ids = lax.broadcasted_iota(jnp.int32, (RIM, qc), 0)
-    for direction, total in ((0, total_f), (1, total_b)):
-        msg[direction, pl.ds(0, DV), :] = total.astype(bf16)
-        log = logs[:, direction * qc : (direction + 1) * qc]
-        hi = log.astype(bf16).astype(f32)
-        lo = log - hi
-        msg[direction, pl.ds(DV, RIM), :] = jnp.where(
-            ids == 0, hi, jnp.where(ids == 1, lo, 0.0)
-        ).astype(bf16)
+
+    def packed(*values):
+        filled = jnp.zeros((RIM, qc), f32)
+        for i, value in enumerate(values):
+            hi = value.astype(bf16).astype(f32)
+            filled = jnp.where(ids == 2 * i, hi, jnp.where(ids == 2 * i + 1, value - hi, filled))
+        return filled.astype(bf16)
+
+    pair_out[pl.ds(0, hd), :] = total[0, other_half, :].astype(bf16)
+    pair_out[pl.ds(hd, hd), :] = total[1, other_half, :].astype(bf16)
+    pair_out[pl.ds(2 * hd, RIM), :] = packed(log_f, log_b)
+
+    def pair_copy(i):
+        return pltpu.make_async_remote_copy(
+            src_ref=(pair_out, back_out)[i],
+            dst_ref=(pair_in, back_in)[i],
+            send_sem=pair_send.at[i],
+            recv_sem=pair_recv.at[i],
+            device_id={"sp": me + 1 - 2 * odd},
+            device_id_type=MESH,
+        )
 
     def state_copy(d):
-        peer = lax.rem(me + d, n)
+        peer = lax.rem(plane + d, planes)
         return pltpu.make_async_remote_copy(
-            src_ref=msg.at[jnp.where(peer > me, 0, 1)],
-            dst_ref=inbox.at[me],
+            src_ref=msg.at[jnp.where(peer > plane, 0, 1)],
+            dst_ref=inbox.at[plane],
             send_sem=st_send.at[d - 1],
             recv_sem=st_recv.at[d - 1],
-            device_id={"sp": peer},
+            device_id={"sp": 2 * peer + odd},
             device_id_type=MESH,
         )
 
     def state_landed(source):
-        d = lax.rem(me - source + n, n)
+        d = lax.rem(plane - source + planes, planes)
         return pltpu.make_async_remote_copy(
             src_ref=msg.at[0],
             dst_ref=inbox.at[source],
             send_sem=st_send.at[d - 1],
             recv_sem=st_recv.at[d - 1],
-            device_id={"sp": source},
+            device_id={"sp": 2 * source + odd},
             device_id_type=MESH,
         )
 
-    for d in range(1, n):
+    pair_copy(0).start()
+    pump(PUMPS[0])
+    pair_copy(0).wait_recv()
+    even = odd == 0
+    theirs_f = pair_in[pl.ds(0, hd), :].astype(f32)
+    theirs_b = pair_in[pl.ds(hd, hd), :].astype(f32)
+    tail = pair_in[pl.ds(2 * hd, RIM), :].astype(f32)
+    peer_log_f, peer_log_b = tail[0:1] + tail[1:2], tail[2:3] + tail[3:4]
+    mine_f, mine_b = total[0, my_half, :], total[1, my_half, :]
+    late_f = jnp.exp(jnp.where(even, peer_log_f, log_f))
+    late_b = jnp.exp(jnp.where(even, log_b, peer_log_b))
+    msg[0, pl.ds(0, hd), :] = (
+        late_f * jnp.where(even, mine_f, theirs_f) + jnp.where(even, theirs_f, mine_f)
+    ).astype(bf16)
+    msg[1, pl.ds(0, hd), :] = (
+        late_b * jnp.where(even, theirs_b, mine_b) + jnp.where(even, mine_b, theirs_b)
+    ).astype(bf16)
+    msg[0, pl.ds(hd, RIM), :] = packed(log_f + peer_log_f)
+    msg[1, pl.ds(hd, RIM), :] = packed(log_b + peer_log_b)
+    for d in range(1, planes):
         state_copy(d).start()
+    pump(PUMPS[1])
+
+    def join(source, state):
+        state_landed(source).wait_recv()
+        tail = inbox[source, pl.ds(hd, RIM), :].astype(f32)
+        log = tail[0:1, :] + tail[1:2, :]
+        return jnp.exp(log) * state + inbox[source, pl.ds(0, hd), :].astype(f32)
+
+    entry[0] = start[0].T
+    entry[1] = start[1].T
+    plane_f = lax.fori_loop(0, plane, join, entry[0, my_half, :])
+    plane_b = lax.fori_loop(
+        0, planes - 1 - plane, lambda i, st: join(planes - 1 - i, st), entry[1, my_half, :]
+    )
+    after_mine_f = jnp.exp(log_f) * plane_f + mine_f
+    after_theirs_f = jnp.exp(peer_log_f) * plane_f + theirs_f
+    after_mine_b = jnp.exp(log_b) * plane_b + mine_b
+    after_theirs_b = jnp.exp(peer_log_b) * plane_b + theirs_b
+    back_out[pl.ds(0, hd), :] = jnp.where(even, after_mine_f, plane_f).astype(bf16)
+    back_out[pl.ds(hd, hd), :] = jnp.where(even, plane_b, after_mine_b).astype(bf16)
+    pair_copy(1).start()
+    entry[0, my_half, :] = jnp.where(even, plane_f, after_theirs_f)
+    entry[1, my_half, :] = jnp.where(even, after_theirs_b, plane_b)
 
     pump_to((POOL, half, CHUNKS // 2 - 1))
     pbuf[pl.ds(RIM, seq), :] = nn(normed[...], wpl[...]).astype(bf16)
@@ -601,15 +678,10 @@
         pbuf[pl.ds(RIM + seq, RIM), :] = jnp.zeros((RIM, pc), bf16)
 
     pump(1)
-
-    def join(source, state):
-        state_landed(source).wait_recv()
-        tail = inbox[source, pl.ds(DV, RIM), :].astype(f32)
-        log = tail[0:1, :] + tail[1:2, :]
-        return jnp.exp(log) * state + inbox[source, pl.ds(0, DV), :].astype(f32)
-
-    state_f = lax.fori_loop(0, me, join, start[0].T)
-    state_b = lax.fori_loop(0, n - 1 - me, lambda i, st: join(n - 1 - i, st), start[1].T)
+    pair_copy(1).wait_recv()
+    entry[0, other_half, :] = back_in[pl.ds(0, hd), :].astype(f32)
+    entry[1, other_half, :] = back_in[pl.ds(hd, hd), :].astype(f32)
+    state_f, state_b = entry[0], entry[1]
     for b in reversed(range(blocks)):
         before_b[b] = state_b
         state_b = jnp.exp(edges[b : b + 1, qc:]) * state_b + upd[b, :, qc:]
@@ -742,7 +814,9 @@
     def _():
         halo(1).wait_send()
 
-    for d in range(1, n):
+    for i in range(2):
+        pair_copy(i).wait_send()
+    for d in range(1, planes):
         state_copy(d).wait_send()
     for i in range(n):
         sib_copy(i).wait_send()
@@ -798,10 +872,15 @@
     dma = pltpu.SemaphoreType.DMA
     return pl.pallas_call(
         functools.partial(fused, n),
-        out_shape=jax.ShapeDtypeStruct((m, n * ocols), bf16),
-        in_specs=[hbm] * 5 + [vmem] * 5 + [hbm] * 3,
+        out_shape=pltpu.VMEM((m, n * ocols), bf16),
+        in_specs=[hbm] * 13,
         out_specs=vmem,
         scratch_shapes=[
+            pltpu.VMEM((decay_inner_weight.shape[1], width), bf16),
+            pltpu.VMEM((2, RANK, decay_outer_weight.shape[2]), bf16),
+            pltpu.VMEM(channel_decay_bias.shape, f32),
+            pltpu.VMEM(spike_log_decay.shape, f32),
+            pltpu.VMEM((2, qc, DV), f32),
             pltpu.VMEM((seq, width), bf16),
             pltpu.VMEM((seq, width), bf16),
             pltpu.VMEM((width, 2 * qc + vc), bf16),
@@ -816,8 +895,14 @@
             pltpu.VMEM((blocks, DV, qc), f32),
             pltpu.VMEM((seq, vc), f32),
             pltpu.VMEM((seq, pc + vc), bf16),
-            pltpu.VMEM((2, DV + RIM, qc), bf16),
-            pltpu.VMEM((n, DV + RIM, qc), bf16),
+            pltpu.VMEM((2, DV, qc), f32),
+            pltpu.VMEM((DV + RIM, qc), bf16),
+            pltpu.VMEM((DV + RIM, qc), bf16),
+            pltpu.VMEM((2, DV // 2 + RIM, qc), bf16),
+            pltpu.VMEM((n // 2, DV // 2 + RIM, qc), bf16),
+            pltpu.VMEM((DV, qc), bf16),
+            pltpu.VMEM((DV, qc), bf16),
+            pltpu.VMEM((2, DV, qc), f32),
             pltpu.VMEM((pc, pc), bf16),
             pltpu.VMEM((n, 2 * m, ocols), bf16),
             pltpu.VMEM((n, 2 * m, ocols), bf16),
@@ -825,15 +910,17 @@
             pltpu.VMEM((n, m, ocols), bf16),
             pltpu.VMEM((n, m, ocols), bf16),
             pltpu.VMEM((n, m, ocols), f32),
-            dma((8,)),
+            dma((13,)),
             dma((1 + 2 * TOK_CHUNKS,)),
             dma((1 + 2 * TOK_CHUNKS,)),
             dma((3, 2, CHUNKS, n // 2)),
             dma((3, 2, CHUNKS, n // 2)),
             dma((2,)),
             dma((2,)),
-            dma((n - 1,)),
-            dma((n - 1,)),
+            dma((2,)),
+            dma((2,)),
+            dma((n // 2 - 1,)),
+            dma((n // 2 - 1,)),
             dma((n,)),
             dma((n,)),
             dma((n,)),

time: 79.4 us -> 71.2 us (0.90)
  Pallas kernels: 77.3 us -> 70.3 us
  local copies, waits for them, and re-layouts: 1.88 us -> 0.8 us
    pallas_call x1, Pallas kernels: 77.3 us -> 70.3 us  [one_kernel(): pl.pallas_call(functools.partial(fused, n), out_shape=pltpu.VMEM((m, n *...]
    unnamed x1, local copies, waits for them, and re-layouts: 1.88 us -> 0.8 us
where the time goes in v2:
time: 71.2 us; the launch traced here: 71.1 us
  Pallas kernels  70.3 us (99%)
  local copies, waits for them, and re-layouts  0.8 us (1%)
    pallas_call x1, Pallas kernels, one_kernel(): pl.pallas_call(functools.partial(fused, n), out_shape=pltpu.VMEM((m, n *...  70.3 us

profile of v2, /device:TPU:0, one launch (start us, length us, event | category | flops | bytes accessed | tf_op | source)
XLA Modules:
  0.0 71.1 jit_solution(2050470926808550178)
XLA Ops:
  0.0 70.3 %shard_map.127 = bf16[128,2048]{1,0:T(8,128)(2,1)S(1)} custom-call(bf16[128,2048]{1,0:T(8,128)(2,1)} %tokens.1, bf16[256,256]{1,0:T(8,128)(2,1)} %w_pool.1, bf16[256,128]{1,0:T(8,128)(2,1)} %w_query.1, bf16[256,128]{1,0:T(8,128)(2,1)} %w_key.1, bf16[256,256]{1,0:T(8,128)(2,1)} %w_value.1, bf16[64,2048]{1,0:T(8,128)(2,1)} %bitcast.2, ...), custom_call_target="tpu_custom_call" | custom-call | tf_op jit(solution)/shard_map/pallas_call | solution.py:873
  70.3 0.8 %copy.15 = bf16[128,2048]{1,0:T(8,128)(2,1)} copy(bf16[128,2048]{1,0:T(8,128)(2,1)S(1)} %shard_map.127) | data formatting | bytes 1048576

commit v3 on v2

--- a/solution.py
+++ b/solution.py
@@ -235,10 +235,10 @@
 
 MESH = pl.DeviceIdType.MESH
 CHUNKS = 4
-TOK_CHUNKS = 4
+TOK_CHUNKS = 8
 RIM = 16
-QKV, POOL, OUT = range(3)
-PUMPS = (3, 4)
+KV, QP, OUT = range(3)
+PUMPS = (3, 7)
 
 
 def nt(a, b):
@@ -276,17 +276,16 @@
     start,
     xraw,
     normed,
-    wqkv,
-    wpl,
+    wkv,
+    wqp,
     obuf,
     pbuf,
-    qkv,
+    kv,
     ld,
-    qbuf,
+    kbuf,
     upd,
     edges,
     before_b,
-    acc,
     act,
     total,
     pair_out,
@@ -362,13 +361,13 @@
     my_rows = pl.ds(pl.multiple_of(me * rows, rows), rows)
     my_tok = pl.ds(pl.multiple_of(tp * m, m), m)
     w_copies = [
-        local(w_query, wqkv.at[my_rows, pl.ds(0, qc)]),
-        local(w_key, wqkv.at[my_rows, pl.ds(qc, qc)]),
-        local(w_value, wqkv.at[my_rows, pl.ds(2 * qc, vc)]),
+        local(w_key, wkv.at[my_rows, pl.ds(0, qc)]),
+        local(w_value, wkv.at[my_rows, pl.ds(qc, vc)]),
     ]
     t_copy = local(tokens, xraw.at[my_tok])
     late_copies = [
-        local(w_pool, wpl.at[my_rows]),
+        local(w_query, wqp.at[my_rows, pl.ds(0, qc)]),
+        local(w_pool, wqp.at[my_rows, pl.ds(qc, pc)]),
         local(w_pool_out, obuf.at[me, pl.ds(0, pc)]),
         local(w_att_out, obuf.at[me, pl.ds(pc, vc)]),
         local(group_map.at[tp], gmap),
@@ -392,7 +391,7 @@
         else:
             step = rows // CHUNKS
             at = pl.ds(pl.multiple_of(origin * rows + c * step, step), step)
-            part = wqkv.at[at] if group == QKV else wpl.at[at]
+            part = wkv.at[at] if group == KV else wqp.at[at]
         return pltpu.make_async_remote_copy(
             src_ref=part,
             dst_ref=part,
@@ -460,7 +459,6 @@
     normalize_rows(tp, 0, m)
     token_copy(0).wait_recv()
     normalize_rows(sibling, 0, m)
-    pump(1)
     for c in range(TOK_CHUNKS):
         token_copy(1, c).wait_recv()
         token_copy(2, c).start()
@@ -468,9 +466,10 @@
         if c > 0:
             token_copy(2, c - 1).wait_recv()
             normalize_rows(across_sibling, c - 1, m // TOK_CHUNKS)
-        pump(2)
+        pump(1)
     token_copy(2, TOK_CHUNKS - 1).wait_recv()
     normalize_rows(across_sibling, TOK_CHUNKS - 1, m // TOK_CHUNKS)
+    pump(CHUNKS // 2 + CHUNKS)
 
     low = nt(normed[...], inner[...]).astype(bf16)
     cols = pl.ds(pl.multiple_of(tp * qc, qc), qc)
@@ -492,8 +491,8 @@
             jnp.minimum(pre, 0.0) - jnp.log1p(jnp.exp(-jnp.abs(pre)))
         ) / gate_norm_factor + spread
 
-    pump_to((QKV, half, CHUNKS // 2 - 1))
-    qkv[...] = nn(normed[...], wqkv[...]).astype(bf16)
+    pump_to((KV, half, CHUNKS // 2 - 1))
+    kv[...] = nn(normed[...], wkv[...]).astype(bf16)
     pump(1)
 
     row_ids = lax.broadcasted_iota(jnp.int32, (BLOCK, BLOCK), 0)
@@ -515,28 +514,18 @@
         at = pl.ds(b * BLOCK, BLOCK)
         cum_f = jnp.dot(lower, ld[at, :qc], precision=highest, preferred_element_type=f32)
         cum_b = jnp.dot(upper, ld[at, qc:], precision=highest, preferred_element_type=f32)
-        q = qkv[at, :qc].astype(f32) * KEY_CHANNELS ** (-0.5)
-        k = qkv[at, qc : 2 * qc].astype(f32)
-        v = qkv[at, 2 * qc :]
-        vf = v.astype(f32)
-        qf = (q * jnp.exp(cum_f)).astype(bf16)
-        qb = (q * jnp.exp(cum_b)).astype(bf16)
-        kf = k * jnp.exp(-cum_f)
-        kb = k * jnp.exp(-cum_b)
+        k = kv[at, :qc].astype(f32)
         edge_f = cum_f[BLOCK - 1 : BLOCK, :]
         edge_b = cum_b[0:1, :]
+        ld[at, :qc] = cum_f
+        ld[at, qc:] = cum_b
+        kbuf[at, :qc] = (k * jnp.exp(-cum_f)).astype(bf16)
+        kbuf[at, qc:] = (k * jnp.exp(-cum_b)).astype(bf16)
+        edges[b : b + 1, :] = jnp.concatenate([edge_f, edge_b], axis=1)
         weighted = jnp.concatenate(
             [k * jnp.exp(edge_f - cum_f), k * jnp.exp(edge_b - cum_b)], axis=1
         ).astype(bf16)
-        qbuf[at, :qc] = qf
-        qbuf[at, qc:] = qb
-        edges[b : b + 1, :] = jnp.concatenate([edge_f, edge_b], axis=1)
-        scores_f = nt(qf, jnp.concatenate([kf * k0, kf * k1], axis=0).astype(bf16))
-        scores_b = nt(qb, jnp.concatenate([kb * k0, kb * k1], axis=0).astype(bf16))
-        scores = jnp.where(allowed, scores_f, scores_b).astype(bf16)
-        both = jnp.concatenate([vf * v0, vf * v1], axis=0).astype(bf16)
-        acc[at, :] = nn(scores, both)
-        full = tn(v, weighted)
+        full = tn(kv[at, qc:], weighted)
         upd[b] = jnp.where(first2, full[:DV], full[DV:])
         if b % 4 == 3:
             pump(1)
@@ -645,8 +634,8 @@
     entry[0, my_half, :] = jnp.where(even, plane_f, after_theirs_f)
     entry[1, my_half, :] = jnp.where(even, after_theirs_b, plane_b)
 
-    pump_to((POOL, half, CHUNKS // 2 - 1))
-    pbuf[pl.ds(RIM, seq), :] = nn(normed[...], wpl[...]).astype(bf16)
+    pump_to((QP, half, CHUNKS // 2 - 1))
+    pbuf[pl.ds(RIM, seq), :] = nn(normed[...], wqp[:, qc:]).astype(bf16)
 
     def halo(side):
         src = pl.ds(seq, RIM) if side == 0 else pl.ds(RIM, RIM)
@@ -677,6 +666,7 @@
     def _():
         pbuf[pl.ds(RIM + seq, RIM), :] = jnp.zeros((RIM, pc), bf16)
 
+    query = nn(normed[...], wqp[:, :qc]).astype(bf16)
     pump(1)
     pair_copy(1).wait_recv()
     entry[0, other_half, :] = back_in[pl.ds(0, hd), :].astype(f32)
@@ -687,6 +677,16 @@
         state_b = jnp.exp(edges[b : b + 1, qc:]) * state_b + upd[b, :, qc:]
     for b in range(blocks):
         at = pl.ds(b * BLOCK, BLOCK)
+        q = query[b * BLOCK : (b + 1) * BLOCK].astype(f32) * KEY_CHANNELS ** (-0.5)
+        qf = (q * jnp.exp(ld[at, :qc])).astype(bf16)
+        qb = (q * jnp.exp(ld[at, qc:])).astype(bf16)
+        kf = kbuf[at, :qc].astype(f32)
+        kb = kbuf[at, qc:].astype(f32)
+        scores_f = nt(qf, jnp.concatenate([kf * k0, kf * k1], axis=0).astype(bf16))
+        scores_b = nt(qb, jnp.concatenate([kb * k0, kb * k1], axis=0).astype(bf16))
+        scores = jnp.where(allowed, scores_f, scores_b).astype(bf16)
+        vf = kv[at, qc:].astype(f32)
+        both = jnp.concatenate([vf * v0, vf * v1], axis=0).astype(bf16)
         back = before_b[b]
         memory = jnp.concatenate(
             [
@@ -695,14 +695,15 @@
             ],
             axis=0,
         ).astype(bf16)
-        joined = acc[at, :] + nt(qbuf[at, :], memory)
+        joined = nn(scores, both) + nt(jnp.concatenate([qf, qb], axis=1), memory)
         for h in range(vc // DV):
             o = joined[:, h * DV : (h + 1) * DV]
             scale = lax.rsqrt(jnp.mean(o * o, axis=-1, keepdims=True) + eps_value)
             act[at, pc + h * DV : pc + (h + 1) * DV] = (o * scale).astype(bf16)
         if b + 1 < blocks:
             state_f = jnp.exp(edges[b : b + 1, :qc]) * state_f + upd[b, :, :qc]
-    pump(1)
+        if b % 4 == 3:
+            pump(1)
 
     @pl.when(me > 0)
     def _():
@@ -825,22 +826,15 @@
 
 def event_order(half):
     lead, rest = range(CHUNKS // 2), range(CHUNKS // 2, CHUNKS)
-    events = [(QKV, s, i) for s in range(half - 1) for i in range(CHUNKS)]
-    events += [(QKV, half - 1, i) for i in lead]
-    events += [(POOL, 0, i) for i in range(CHUNKS)]
-    events += [(QKV, half - 1, i) for i in rest]
-    events += [(QKV, half, i) for i in lead]
-    events += [(OUT, 0, 0)]
-    for s in range(1, half - 1):
-        events += [(POOL, s, i) for i in range(CHUNKS)] + [(OUT, 0, s)] * (s < CHUNKS)
-    events += [(POOL, half - 1, i) for i in lead]
-    events += [(OUT, 0, i) for i in range(half - 1, CHUNKS)]
-    events += [(POOL, half - 1, i) for i in rest]
-    events += [(POOL, half, i) for i in lead]
-    for s in range(1, half - 1):
-        events += [(OUT, s, i) for i in range(CHUNKS)]
-    events += [(OUT, half - 1, i) for i in range(CHUNKS)]
-    events += [(OUT, half, i) for i in lead]
+    events = []
+    for group in (KV, QP, OUT):
+        waits = events[-CHUNKS:] if events else []
+        events = events[: len(events) - len(waits)]
+        events += [(group, 0, i) for i in range(CHUNKS)] + waits
+        for s in range(1, half - 1):
+            events += [(group, s, i) for i in range(CHUNKS)]
+        events += [(group, half - 1, i) for i in lead]
+        events += [(group, half - 1, i) for i in rest] + [(group, half, i) for i in lead]
     return events
 
 
@@ -883,17 +877,16 @@
             pltpu.VMEM((2, qc, DV), f32),
             pltpu.VMEM((seq, width), bf16),
             pltpu.VMEM((seq, width), bf16),
-            pltpu.VMEM((width, 2 * qc + vc), bf16),
-            pltpu.VMEM((width, pc), bf16),
+            pltpu.VMEM((width, qc + vc), bf16),
+            pltpu.VMEM((width, qc + pc), bf16),
             pltpu.VMEM((n, pc + vc, ocols), bf16),
             pltpu.VMEM((seq + 2 * RIM, pc), bf16),
-            pltpu.VMEM((seq, 2 * qc + vc), bf16),
+            pltpu.VMEM((seq, qc + vc), bf16),
             pltpu.VMEM((seq, 2 * qc), f32),
             pltpu.VMEM((seq, 2 * qc), bf16),
             pltpu.VMEM((blocks, DV, 2 * qc), f32),
             pltpu.VMEM((blocks, 2 * qc), f32),
             pltpu.VMEM((blocks, DV, qc), f32),
-            pltpu.VMEM((seq, vc), f32),
             pltpu.VMEM((seq, pc + vc), bf16),
             pltpu.VMEM((2, DV, qc), f32),
             pltpu.VMEM((DV + RIM, qc), bf16),

time: 71.2 us -> 67.2 us (0.944)
  Pallas kernels: 70.3 us -> 66.3 us
    pallas_call x1, Pallas kernels: 70.3 us -> 66.3 us  [one_kernel(): pl.pallas_call(functools.partial(fused, n), out_shape=pltpu.VMEM((m, n *...]
where the time goes in v3:
time: 67.2 us; the launch traced here: 67.1 us
  Pallas kernels  66.3 us (99%)
  local copies, waits for them, and re-layouts  0.8 us (1%)
    pallas_call x1, Pallas kernels, one_kernel(): pl.pallas_call(functools.partial(fused, n), out_shape=pltpu.VMEM((m, n *...  66.3 us

profile of v3, /device:TPU:0, one launch (start us, length us, event | category | flops | bytes accessed | tf_op | source)
XLA Modules:
  0.0 67.1 jit_solution(18438517323251980370)
XLA Ops:
  0.0 66.3 %shard_map.127 = bf16[128,2048]{1,0:T(8,128)(2,1)S(1)} custom-call(bf16[128,2048]{1,0:T(8,128)(2,1)} %tokens.1, bf16[256,256]{1,0:T(8,128)(2,1)} %w_pool.1, bf16[256,128]{1,0:T(8,128)(2,1)} %w_query.1, bf16[256,128]{1,0:T(8,128)(2,1)} %w_key.1, bf16[256,256]{1,0:T(8,128)(2,1)} %w_value.1, bf16[64,2048]{1,0:T(8,128)(2,1)} %bitcast.2, ...), custom_call_target="tpu_custom_call" | custom-call | tf_op jit(solution)/shard_map/pallas_call | solution.py:867
  66.3 0.8 %copy.15 = bf16[128,2048]{1,0:T(8,128)(2,1)} copy(bf16[128,2048]{1,0:T(8,128)(2,1)S(1)} %shard_map.127) | data formatting | bytes 1048576

commit v4 on v3

--- a/solution.py
+++ b/solution.py
@@ -239,6 +239,8 @@
 RIM = 16
 KV, QP, OUT = range(3)
 PUMPS = (3, 7)
+TOK_PUMPS = (3, 0, 1, 2, 0, 2, 1, 5)
+LAG = 3
 
 
 def nt(a, b):
@@ -302,6 +304,8 @@
     x_out,
     x_in,
     own,
+    d_out,
+    d_in,
     local_sem,
     tok_send,
     tok_recv,
@@ -317,6 +321,8 @@
     sib_recv,
     x_send,
     x_recv,
+    d_send,
+    d_recv,
 ):
     me = lax.axis_index("sp")
     tp = lax.axis_index("tp")
@@ -325,7 +331,8 @@
     seq = normed.shape[0]
     rows = w_pool.shape[0]
     pc, qc, vc = w_pool.shape[1], w_query.shape[1], w_value.shape[1]
-    ocols = obuf.shape[2]
+    hcols = obuf.shape[3]
+    ocols = 2 * hcols
     blocks = seq // BLOCK
     half = n // 2
     f32, bf16 = jnp.float32, jnp.bfloat16
@@ -368,8 +375,10 @@
     late_copies = [
         local(w_query, wqp.at[my_rows, pl.ds(0, qc)]),
         local(w_pool, wqp.at[my_rows, pl.ds(qc, pc)]),
-        local(w_pool_out, obuf.at[me, pl.ds(0, pc)]),
-        local(w_att_out, obuf.at[me, pl.ds(pc, vc)]),
+        local(w_pool_out.at[:, pl.ds(0, hcols)], obuf.at[me, 0, pl.ds(0, pc)]),
+        local(w_pool_out.at[:, pl.ds(hcols, hcols)], obuf.at[me, 1, pl.ds(0, pc)]),
+        local(w_att_out.at[:, pl.ds(0, hcols)], obuf.at[me, 0, pl.ds(pc, vc)]),
+        local(w_att_out.at[:, pl.ds(hcols, hcols)], obuf.at[me, 1, pl.ds(pc, vc)]),
         local(group_map.at[tp], gmap),
         local(inner_in, inner),
         local(outer_in, outer),
@@ -386,8 +395,9 @@
         shift = s + 1 if landed else s
         origin = origins[-shift if d == 0 else shift]
         if group == OUT:
-            step = (pc + vc) // CHUNKS
-            part = obuf.at[origin, pl.ds(c * step, step)]
+            per = CHUNKS // 2
+            step = (pc + vc) // per
+            part = obuf.at[origin, c // per, pl.ds(c % per * step, step)]
         else:
             step = rows // CHUNKS
             at = pl.ds(pl.multiple_of(origin * rows + c * step, step), step)
@@ -459,17 +469,21 @@
     normalize_rows(tp, 0, m)
     token_copy(0).wait_recv()
     normalize_rows(sibling, 0, m)
+    part = m // TOK_CHUNKS
+
+    def relayed(c):
+        token_copy(2, c).wait_recv()
+        normalize_rows(across_sibling, c, part)
+
     for c in range(TOK_CHUNKS):
+        pump(TOK_PUMPS[c])
         token_copy(1, c).wait_recv()
         token_copy(2, c).start()
-        normalize_rows(across, c, m // TOK_CHUNKS)
-        if c > 0:
-            token_copy(2, c - 1).wait_recv()
-            normalize_rows(across_sibling, c - 1, m // TOK_CHUNKS)
-        pump(1)
-    token_copy(2, TOK_CHUNKS - 1).wait_recv()
-    normalize_rows(across_sibling, TOK_CHUNKS - 1, m // TOK_CHUNKS)
-    pump(CHUNKS // 2 + CHUNKS)
+        normalize_rows(across, c, part)
+        if c >= LAG:
+            relayed(c - LAG)
+    for c in range(TOK_CHUNKS - LAG, TOK_CHUNKS):
+        relayed(c)
 
     low = nt(normed[...], inner[...]).astype(bf16)
     cols = pl.ds(pl.multiple_of(tp * qc, qc), qc)
@@ -732,95 +746,164 @@
         pooled = (sums / counted - pbuf[pl.ds(RIM + b * tile, tile), :].astype(f32)).astype(bf16)
         act[pl.ds(b * tile, tile), :pc] = nn(pooled, gmap[...]).astype(bf16)
 
-    block_at = [0]
-    for k in range(1, half):
-        block_at += [-k, k]
-    block_at.append(half)
+    units = [(0, None)]
+    for k in range(1, half - 1):
+        units += [(-k, None), (k, None)]
+    units += [(1 - half, 0), (half - 1, 1), (1 - half, 1), (half - 1, 0), (half, 0), (half, 1)]
+    direct = len(units) - 2
+
+    def lanes(i):
+        return pl.ds(0, ocols if units[i][1] is None else hcols)
 
     def rows_of(dest):
         return pl.ds(pl.multiple_of(dest * m, m), m)
 
-    def sib_copy(i):
+    def sib_copy(i, part):
+        at = (i, pl.ds(part * m, m), lanes(i))
         return pltpu.make_async_remote_copy(
-            src_ref=sib_out.at[i],
-            dst_ref=sib_in.at[i],
-            send_sem=sib_send.at[i],
-            recv_sem=sib_recv.at[i],
+            src_ref=sib_out.at[at],
+            dst_ref=sib_in.at[at],
+            send_sem=sib_send.at[i, part],
+            recv_sem=sib_recv.at[i, part],
             device_id={"tp": sibling},
             device_id_type=MESH,
         )
 
     def x_copy(i):
+        at = (i, slice(None), lanes(i))
         return pltpu.make_async_remote_copy(
-            src_ref=x_out.at[i],
-            dst_ref=x_in.at[i],
+            src_ref=x_out.at[at],
+            dst_ref=x_in.at[at],
             send_sem=x_send.at[i],
             recv_sem=x_recv.at[i],
             device_id={"tp": across},
             device_id_type=MESH,
         )
 
+    def direct_copy():
+        return pltpu.make_async_remote_copy(
+            src_ref=d_out,
+            dst_ref=d_in,
+            send_sem=d_send.at[0],
+            recv_sem=d_recv.at[0],
+            device_id={"tp": across_sibling},
+            device_id_type=MESH,
+        )
+
     def produce(i):
-        weights = obuf[origins[block_at[i]]]
-        sib_out[i, pl.ds(0, m)] = nn(act[rows_of(across_sibling), :], weights).astype(bf16)
-        sib_out[i, pl.ds(m, m)] = nn(act[rows_of(sibling), :], weights).astype(bf16)
-        sib_copy(i).start()
-        x_part[i] = nn(act[rows_of(across), :], weights)
-        own[i] = nn(act[rows_of(tp), :], weights)
+        offset, side = units[i]
+        source = origins[offset]
+        if side is None:
+            weights = jnp.concatenate([obuf[source, 0], obuf[source, 1]], axis=1)
+        else:
+            weights = obuf[source, side]
+        far = nn(act[rows_of(across_sibling), :], weights).astype(bf16)
+        if i == direct:
+            d_out[...] = far
+            direct_copy().start()
+            x_out[i, :, lanes(i)] = nn(act[rows_of(across), :], weights).astype(bf16)
+            x_copy(i).start()
+        else:
+            sib_out[i, pl.ds(0, m), lanes(i)] = far
+            sib_copy(i, 0).start()
+            x_part[i, :, lanes(i)] = nn(act[rows_of(across), :], weights)
+        sib_out[i, pl.ds(m, m), lanes(i)] = nn(act[rows_of(sibling), :], weights).astype(bf16)
+        sib_copy(i, 1).start()
+        own[i, :, lanes(i)] = nn(act[rows_of(tp), :], weights)
 
     def cross(i):
-        sib_copy(i).wait_recv()
-        x_out[i] = (x_part[i] + sib_in[i, pl.ds(0, m)].astype(f32)).astype(bf16)
+        sib_copy(i, 0).wait_recv()
+        x_out[i, :, lanes(i)] = (
+            x_part[i, :, lanes(i)] + sib_in[i, pl.ds(0, m), lanes(i)].astype(f32)
+        ).astype(bf16)
         x_copy(i).start()
 
     def finish(i):
+        offset, side = units[i]
+        sib_copy(i, 1).wait_recv()
         x_copy(i).wait_recv()
-        at = pl.ds(pl.multiple_of(origins[block_at[i]] * ocols, ocols), ocols)
-        result[:, at] = (
-            own[i] + sib_in[i, pl.ds(m, m)].astype(f32) + x_in[i].astype(f32)
-        ).astype(bf16)
-
+        summed = (
+            own[i, :, lanes(i)]
+            + sib_in[i, pl.ds(m, m), lanes(i)].astype(f32)
+            + x_in[i, :, lanes(i)].astype(f32)
+        )
+        if i == direct:
+            direct_copy().wait_recv()
+            summed = summed + d_in[...].astype(f32)
+        begin = origins[offset] * ocols + (side or 0) * hcols
+        width = ocols if side is None else hcols
+        result[:, pl.ds(pl.multiple_of(begin, width), width)] = summed.astype(bf16)
+
+    def send_waits():
+        token_copy(0).wait_send()
+        for c in range(TOK_CHUNKS):
+            token_copy(1, c).wait_send()
+            token_copy(2, c).wait_send()
+        for group in range(2):
+            for d in range(2):
+                for c in range(CHUNKS):
+                    for s in range(hops_of(d, c)):
+                        ring_copy(group, d, c, s, False).wait_send()
+
+        @pl.when(me < n - 1)
+        def _():
+            halo(0).wait_send()
+
+        @pl.when(me > 0)
+        def _():
+            halo(1).wait_send()
+
+        for i in range(2):
+            pair_copy(i).wait_send()
+        for d in range(1, planes):
+            state_copy(d).wait_send()
+
+    last = len(units)
+    whole = last - 6
+    pump(1)
     produce(0)
-    for s in range(1, half):
+    for s in range(1, half - 1):
         pump_to((OUT, s, CHUNKS - 1))
         produce(2 * s - 1)
         cross(2 * s - 2)
+        if s == 1:
+            pump(1)
         produce(2 * s)
         cross(2 * s - 1)
-        if s > 1:
-            finish(2 * s - 4)
-            finish(2 * s - 3)
+    pump_to((OUT, half - 1, CHUNKS // 2 - 1))
+    cross(whole - 1)
+    produce(whole)
+    produce(whole + 1)
+    for i in range(whole - 1):
+        finish(i)
+    cross(whole)
+    cross(whole + 1)
+    pump_to((OUT, half - 1, CHUNKS - 1))
+    produce(whole + 2)
+    produce(whole + 3)
+    send_waits()
+    finish(whole - 1)
+    cross(whole + 2)
+    cross(whole + 3)
     pump(len(order))
-    produce(n - 1)
-    cross(n - 2)
-    cross(n - 1)
-    for i in range(n - 4, n):
+    produce(direct)
+    produce(direct + 1)
+    finish(whole)
+    finish(whole + 1)
+    cross(direct + 1)
+    for i in range(whole + 2, last):
         finish(i)
 
-    token_copy(0).wait_send()
-    for c in range(TOK_CHUNKS):
-        token_copy(1, c).wait_send()
-        token_copy(2, c).wait_send()
-    for group in range(3):
-        for d in range(2):
-            for c in range(CHUNKS):
-                for s in range(hops_of(d, c)):
-                    ring_copy(group, d, c, s, False).wait_send()
-
-    @pl.when(me < n - 1)
-    def _():
-        halo(0).wait_send()
-
-    @pl.when(me > 0)
-    def _():
-        halo(1).wait_send()
-
-    for i in range(2):
-        pair_copy(i).wait_send()
-    for d in range(1, planes):
-        state_copy(d).wait_send()
-    for i in range(n):
-        sib_copy(i).wait_send()
+    for d in range(2):
+        for c in range(CHUNKS):
+            for s in range(hops_of(d, c)):
+                ring_copy(OUT, d, c, s, False).wait_send()
+    for i in range(last):
+        if i == direct:
+            direct_copy().wait_send()
+        else:
+            sib_copy(i, 0).wait_send()
+        sib_copy(i, 1).wait_send()
         x_copy(i).wait_send()
 
 
@@ -860,6 +943,7 @@
     pc, qc, vc = (a.shape[1] for a in (pooling_input_weight, query_matrix, value_matrix))
     ocols = pooling_output_weight.shape[1]
     blocks = seq // BLOCK
+    units = n + 3
     f32, bf16 = jnp.float32, jnp.bfloat16
     vmem = pl.BlockSpec(memory_space=pltpu.VMEM)
     hbm = pl.BlockSpec(memory_space=pl.ANY)
@@ -879,7 +963,7 @@
             pltpu.VMEM((seq, width), bf16),
             pltpu.VMEM((width, qc + vc), bf16),
             pltpu.VMEM((width, qc + pc), bf16),
-            pltpu.VMEM((n, pc + vc, ocols), bf16),
+            pltpu.VMEM((n, 2, pc + vc, ocols // 2), bf16),
             pltpu.VMEM((seq + 2 * RIM, pc), bf16),
             pltpu.VMEM((seq, qc + vc), bf16),
             pltpu.VMEM((seq, 2 * qc), f32),
@@ -897,13 +981,15 @@
             pltpu.VMEM((DV, qc), bf16),
             pltpu.VMEM((2, DV, qc), f32),
             pltpu.VMEM((pc, pc), bf16),
-            pltpu.VMEM((n, 2 * m, ocols), bf16),
-            pltpu.VMEM((n, 2 * m, ocols), bf16),
-            pltpu.VMEM((n, m, ocols), f32),
-            pltpu.VMEM((n, m, ocols), bf16),
-            pltpu.VMEM((n, m, ocols), bf16),
-            pltpu.VMEM((n, m, ocols), f32),
-            dma((13,)),
+            pltpu.VMEM((units, 2 * m, ocols), bf16),
+            pltpu.VMEM((units, 2 * m, ocols), bf16),
+            pltpu.VMEM((units, m, ocols), f32),
+            pltpu.VMEM((units, m, ocols), bf16),
+            pltpu.VMEM((units, m, ocols), bf16),
+            pltpu.VMEM((units, m, ocols), f32),
+            pltpu.VMEM((m, ocols // 2), bf16),
+            pltpu.VMEM((m, ocols // 2), bf16),
+            dma((15,)),
             dma((1 + 2 * TOK_CHUNKS,)),
             dma((1 + 2 * TOK_CHUNKS,)),
             dma((3, 2, CHUNKS, n // 2)),
@@ -914,10 +1000,12 @@
             dma((2,)),
             dma((n // 2 - 1,)),
             dma((n // 2 - 1,)),
-            dma((n,)),
-            dma((n,)),
-            dma((n,)),
-            dma((n,)),
+            dma((units, 2)),
+            dma((units, 2)),
+            dma((units,)),
+            dma((units,)),
+            dma((1,)),
+            dma((1,)),
         ],
         compiler_params=pltpu.CompilerParams(
             collective_id=0, has_side_effects=True, vmem_limit_bytes=60 * 2**20

time: 67.2 us -> 65 us (0.967)
  Pallas kernels: 66.3 us -> 64.1 us
    pallas_call x1, Pallas kernels: 66.3 us -> 64.1 us  [one_kernel(): pl.pallas_call(functools.partial(fused, n), out_shape=pltpu.VMEM((m, n *...]
where the time goes in v4:
time: 65 us; the launch traced here: 64.9 us
  Pallas kernels  64.1 us (99%)
  local copies, waits for them, and re-layouts  0.8 us (1%)
    pallas_call x1, Pallas kernels, one_kernel(): pl.pallas_call(functools.partial(fused, n), out_shape=pltpu.VMEM((m, n *...  64.1 us

profile of v4, /device:TPU:0, one launch (start us, length us, event | category | flops | bytes accessed | tf_op | source)
XLA Modules:
  0.0 64.9 jit_solution(5476697734834053706)
XLA Ops:
  0.0 64.1 %shard_map.127 = bf16[128,2048]{1,0:T(8,128)(2,1)S(1)} custom-call(bf16[128,2048]{1,0:T(8,128)(2,1)} %tokens.1, bf16[256,256]{1,0:T(8,128)(2,1)} %w_pool.1, bf16[256,128]{1,0:T(8,128)(2,1)} %w_query.1, bf16[256,128]{1,0:T(8,128)(2,1)} %w_key.1, bf16[256,256]{1,0:T(8,128)(2,1)} %w_value.1, bf16[64,2048]{1,0:T(8,128)(2,1)} %bitcast.2, ...), custom_call_target="tpu_custom_call" | custom-call | tf_op jit(solution)/shard_map/pallas_call | solution.py:951
  64.1 0.8 %copy.15 = bf16[128,2048]{1,0:T(8,128)(2,1)} copy(bf16[128,2048]{1,0:T(8,128)(2,1)S(1)} %shard_map.127) | data formatting | bytes 1048576
